TPU v7x, 32 devices: a whole 2x2x4 slice. The times are simulated.
32 devices in a mesh: ep: 8 (over z, core), tp: 4 (over y, x).
Axes of the slice: x: 2, y: 2, z: 4, core: 2. Of those that a mesh axis runs over, the one named last changes fastest.
Arguments:
- mixer_input: bfloat16 [2048, 1024], P('ep', 'tp'), may hold values from -6 to 6
- log_step: float32 [64], P('tp'), may hold values from -12.8 to -2.7
- decay_shift: float32 [2048, 64], P('ep', 'tp'), may hold values from -2 to 0
- input_map: bfloat16 [2, 64, 64, 16], P(None, 'tp'), may hold values from -71.55418 to 71.55418
- readout: float32 [2, 64, 16, 64], P(None, 'tp'), may hold values from -0.5 to 0.5
- mixer_weight: bfloat16 [1024, 2048], P(None, 'tp'), may hold values from -0.1875 to 0.1875
- expert_input: bfloat16 [1024, 2048], P('ep'), may hold values from -6 to 6
- norm_gain: float32 [2048], replicated, may hold values from 0.1 to 1.9
- routes: int32 [1024, 2], P('ep'), may hold values from 0 to 7, all different within a row; in each aligned block of 128 rows (0 to 127, 128 to 255, ...) at most 64 rows name the same one
- route_weight: float32 [1024, 2], P('ep'), may hold values from 0.1 to 2.5
- expert_switch_matrix: bfloat16 [8, 2048, 4096], P('ep', None, 'tp'), may hold values from -0.125 to 0.125
- up_weight: bfloat16 [8, 2048, 4096], P('ep', None, 'tp'), may hold values from -0.125 to 0.125
- down_weight: bfloat16 [8, 4096, 2048], P('ep', None, 'tp'), may hold values from -0.09375 to 0.09375
- shared_gate: bfloat16 [2048, 1024], P(None, 'tp'), may hold values from -0.125 to 0.125
- shared_up: bfloat16 [2048, 1024], P(None, 'tp'), may hold values from -0.125 to 0.125
- shared_down: bfloat16 [1024, 2048], P(None, 'tp'), may hold values from -0.1875 to 0.1875
Outputs:
- mixer_out: bfloat16 [2048, 2048], P('ep', 'tp')
- experts_out: bfloat16 [1024, 2048], P('ep', 'tp')
Inputs may be any that keep to these rules, and one draw needn't show every extreme that they name: `routes`: each row names 2 different experts. In each aligned block of 128 rows (the rows of one index of ep) no expert is named by more than 64 rows, and in some block one expert is named by exactly 64 rows.
All inputs are finite; a program needn't handle non-finite values.
Results may differ from a plain program's by a relative error of at most 0.0069.
Values may be sent and summed in bfloat16 or wider, within the bound.
A program may use at most 128 MiB of HBM per device.

v0:
```python
import functools

import jax
import jax.numpy as jnp
from jax import lax
from jax.experimental import pallas as pl
from jax.experimental.pallas import tpu as pltpu
from jax.sharding import PartitionSpec as P

MESH = pl.DeviceIdType.MESH
SUBLANES = 8
NT = (((1,), (1,)), ((), ()))


def factors(log_step, states):
    step_rate = jnp.exp(log_step)
    frequency = jnp.pi * jnp.arange(states, dtype=jnp.float32)
    angle = step_rate[:, None] * frequency[None, :]
    turn_cosine = jnp.cos(angle)
    turn_sine = jnp.sin(angle)
    base = jnp.exp(-0.5 * step_rate)[:, None]
    base_real = base * turn_cosine
    starting_quadrature = base * turn_sine
    inverse = 1.0 / (0.25 + frequency * frequency)[None, :]
    lowered = base_real - 1.0
    inject_real = (-0.5 * lowered + starting_quadrature * frequency[None, :]) * inverse
    inject_imaginary = (-0.5 * starting_quadrature - lowered * frequency[None, :]) * inverse
    return (step_rate, turn_cosine, turn_sine, inject_real, inject_imaginary)


def times(ar, ai, br, bi):
    return ar * br - ai * bi, ar * bi + ai * br


def iota(shape, dim):
    return lax.broadcasted_iota(jnp.int32, shape, dim)


def spread(shape, period):
    return (iota(shape, 1) % period == iota(shape, 0)).astype(jnp.bfloat16)


def halves(a):
    high = a.astype(jnp.bfloat16)
    return high, (a - high.astype(jnp.float32)).astype(jnp.bfloat16)


def dot(a, b, dims=None):
    if dims is None:
        return jnp.dot(a, b, preferred_element_type=jnp.float32)
    return lax.dot_general(a, b, dims, preferred_element_type=jnp.float32)


def drive_into(x_ref, rate_ref, shift_ref, map_ref, table_ref, mag, push_re, push_im, states):
    rows, channels = x_ref.shape
    merged = mag.shape[1]
    groups = shift_ref.shape[1]
    width = channels // groups
    steps = rows // SUBLANES
    place = iota((rows, rows), 0)
    order = (iota((rows, rows), 1) == (place % SUBLANES) * steps + place // SUBLANES).astype(
        jnp.bfloat16
    )
    level = jnp.exp(-0.5 * jnp.exp(rate_ref[...]) + shift_ref[...])
    high, rest = halves(level)
    middle = rest
    low = ((level - high.astype(jnp.float32)) - middle.astype(jnp.float32)).astype(jnp.bfloat16)
    widen = (iota((groups, merged), 1) // states == iota((groups, merged), 0)).astype(jnp.bfloat16)
    total = None
    for piece in (high, middle, low):
        part = dot(dot(order, piece).astype(jnp.bfloat16), widen)
        total = part if total is None else total + part
    mag[...] = total
    x = dot(order, x_ref[...]).astype(jnp.bfloat16)
    repeat = spread((width, channels), width)
    mine = iota((merged, channels), 0) // states == iota((merged, channels), 1) // width
    drives = []
    for c in range(2):
        wide = jnp.where(mine, dot(map_ref[c], repeat), 0.0).astype(jnp.bfloat16)
        drives.append(dot(x, wide, NT))
    re, im = times(table_ref[2:3, :], table_ref[3:4, :], drives[0], drives[1])
    push_re[...] = re
    push_im[...] = im


def sweep(table_ref, mag, push_re, push_im, start_re, start_im, keep):
    rows, merged = mag.shape
    turn_re = jnp.broadcast_to(table_ref[0:1, :], (SUBLANES, merged))
    turn_im = jnp.broadcast_to(table_ref[1:2, :], (SUBLANES, merged))

    def one(j, carry):
        re, im, product = carry
        at = pl.ds(pl.multiple_of(j * SUBLANES, SUBLANES), SUBLANES)
        level = mag[at, :]
        next_re, next_im = times(turn_re, turn_im, re, im)
        next_re = level * next_re + push_re[at, :]
        next_im = level * next_im + push_im[at, :]
        if keep:
            push_re[at, :] = next_re
            push_im[at, :] = next_im
        else:
            product = product * level
        return next_re, next_im, product

    product = jnp.ones((SUBLANES, merged), jnp.float32)
    if keep:
        def pair(j, carry):
            return one(j, carry + (None,))[:2]
        return lax.fori_loop(0, rows // SUBLANES, pair, (start_re, start_im))
    return lax.fori_loop(0, rows // SUBLANES, one, (start_re, start_im, product))


def join(table_ref, ends_re, ends_im, product, pre, steps):
    merged = ends_re.shape[1]
    wr, wi = table_ref[0:1, :], table_ref[1:2, :]
    power = 1
    while power < steps:
        wr, wi = times(wr, wi, wr, wi)
        power *= 2
    cr = jnp.zeros((1, merged), jnp.float32)
    ci = cr
    ar = cr + 1.0
    ai = cr
    for s in range(SUBLANES):
        for i, v in enumerate((cr, ci, ar, ai)):
            pre[i, s : s + 1, :] = v
        level = product[s : s + 1]
        fr, fi = level * wr, level * wi
        tr, ti = times(fr, fi, cr, ci)
        cr, ci = tr + ends_re[s : s + 1], ti + ends_im[s : s + 1]
        ar, ai = times(fr, fi, ar, ai)
    return cr, ci, ar, ai


def read_states(readout_ref, push_re, push_im, states):
    rows, merged = push_re.shape
    channels = readout_ref.shape[1]
    width = channels * states // merged
    repeat = spread((states, merged), states)
    mine = iota((channels, merged), 1) // states == iota((channels, merged), 0) // width
    total = None
    for c, ref in enumerate((push_re, push_im)):
        high, low = halves(ref[...])
        back = readout_ref[c] if c == 0 else -readout_ref[c]
        wide_high, wide_low = (
            jnp.where(mine, dot(half, repeat), 0.0).astype(jnp.bfloat16) for half in halves(back)
        )
        part = dot(high, wide_high, NT) + (dot(low, wide_high, NT) + dot(high, wide_low, NT))
        total = part if total is None else total + part
    place = iota((rows, rows), 0)
    steps = rows // SUBLANES
    order = (iota((rows, rows), 1) == (place % steps) * SUBLANES + place // steps).astype(
        jnp.bfloat16
    )
    cube = total + 0.044715 * (total * total * total)
    active = (0.5 * total * (1.0 + jnp.tanh(0.7978845608028654 * cube))).astype(jnp.bfloat16)
    return dot(order, active).astype(jnp.bfloat16)


def remote(src, dst, send, recv, **target):
    return pltpu.make_async_remote_copy(
        src_ref=src, dst_ref=dst, send_sem=send, recv_sem=recv,
        device_id=target, device_id_type=MESH,
    )


def fused_kernel(
    n_ep, n_tp, states,
    x_ref, rate_ref, shift_ref, map_ref, readout_ref, table_ref, weight_ref,
    outgoing, gains, normed, sgate_ref, sup_ref, sdown_ref, gate_hbm, up_hbm, down_hbm,
    out_ref, experts_ref,
    mag, push_re, push_im, pre, summary, active,
    gate, up, down, arrived, hidden, result, returned, shared,
    ep_send, ep_recv, tp_send, tp_recv,
    d_send, d_recv, h_send, h_recv, r_send, r_recv, s_send, s_recv, load,
):
    ep = lax.axis_index("ep")
    tp = lax.axis_index("tp")
    rows, channels = x_ref.shape
    merged = mag.shape[1]
    cap, features = outgoing.shape[1:]
    pair = hidden.shape[2] // cap
    chips = n_ep // pair
    chip = ep // pair
    ff = gate.shape[1]
    columns = down.shape[1]
    barrier = pltpu.get_barrier_semaphore()
    for d in range(1, n_ep):
        pl.semaphore_signal(
            barrier, inc=1, device_id={"ep": lax.rem(ep + d, n_ep)}, device_id_type=MESH
        )
    for d in range(1, n_tp):
        pl.semaphore_signal(
            barrier, inc=1, device_id={"tp": lax.rem(tp + d, n_tp)}, device_id_type=MESH
        )
    loads = [
        pltpu.make_async_copy(hbm.at[0], vmem, load.at[i])
        for i, (hbm, vmem) in enumerate(((gate_hbm, gate), (up_hbm, up), (down_hbm, down)))
    ]
    for copy in loads:
        copy.start()
    sends = []

    def go(copy):
        copy.start()
        sends.append(copy)

    pl.semaphore_wait(barrier, n_ep + n_tp - 2)
    others = [pair * chip + lax.rem(ep + c, pair) for c in range(1, pair)]
    for i in range(1, chips):
        others += [pair * lax.rem(chip + i, chips) + c for c in range(pair)]

    def dispatch(targets):
        for target in targets:
            go(remote(
                outgoing.at[target], arrived.at[ep], d_send.at[target], d_recv.at[ep], ep=target
            ))

    first = 2 * pair - 1
    dispatch(others[:first])
    drive_into(x_ref, rate_ref, shift_ref, map_ref, table_ref, mag, push_re, push_im, states)
    zero = jnp.zeros((SUBLANES, merged), jnp.float32)
    ends_re, ends_im, product = sweep(table_ref, mag, push_re, push_im, zero, zero, False)
    end = join(table_ref, ends_re, ends_im, product, pre, rows // SUBLANES)
    for i, v in enumerate(end):
        summary[ep, i : i + 1, :] = v
    carries = []
    for d in range(1, n_ep):
        copy = remote(
            summary.at[ep], summary.at[ep], ep_send.at[d], ep_recv.at[d],
            ep=lax.rem(ep + d, n_ep),
        )
        go(copy)
        carries.append(copy)
    dispatch(others[first:])
    arrived[ep] = outgoing[ep]

    tokens = normed[...]
    v = dot(tokens, sgate_ref[...])
    shared[tp] = (v / (1.0 + jnp.exp(-v)) * dot(tokens, sup_ref[...])).astype(jnp.bfloat16)
    shares = []
    for d in range(1, n_tp):
        copy = remote(
            shared.at[tp], shared.at[tp], s_send.at[d], s_recv.at[d], tp=lax.rem(tp + d, n_tp)
        )
        go(copy)
        shares.append(copy)

    tile = min(ff, 256)

    def expand(i):
        there = lax.rem(chip + chips - i, chips)
        for c in range(pair):
            if i == 0 and c == 0:
                continue
            source = pair * there + (lax.rem(ep + c, pair) if i == 0 else c)
            remote(
                outgoing.at[source], arrived.at[source], d_send.at[source], d_recv.at[source],
                ep=source,
            ).wait_recv()
        block = pl.ds(pair * there, pair)

        @pl.loop(0, ff // tile)
        def _(n):
            at = pl.ds(pl.multiple_of(n * tile, tile), tile)
            a = arrived[block].reshape(pair * cap, features)
            v = dot(a, gate[:, at])
            hidden[there, tp, :, at] = (
                v / (1.0 + jnp.exp(-v)) * dot(a, up[:, at])
            ).astype(jnp.bfloat16)

        for d in range(1, n_tp):
            q = lax.rem(tp + d, n_tp)
            go(remote(
                hidden.at[there, tp], hidden.at[there, tp], h_send.at[there, q],
                h_recv.at[there, tp], tp=q,
            ))

    for copy in loads[:2]:
        copy.wait()
    expand(0)
    for copy in carries:
        copy.wait_recv()

    def fold(e, carry):
        part = summary[e]
        re, im = times(part[2:3], part[3:4], carry[0], carry[1])
        return re + part[0:1], im + part[1:2]

    nothing = jnp.zeros((1, merged), jnp.float32)
    in_re, in_im = lax.fori_loop(0, ep, fold, (nothing, nothing))
    add_re, add_im = times(pre[2], pre[3], in_re, in_im)
    sweep(table_ref, mag, push_re, push_im, pre[0] + add_re, pre[1] + add_im, True)
    active[tp] = read_states(readout_ref, push_re, push_im, states)
    mixes = []
    for d in range(1, n_tp):
        copy = remote(
            active.at[tp], active.at[tp], tp_send.at[d], tp_recv.at[d], tp=lax.rem(tp + d, n_tp)
        )
        go(copy)
        mixes.append(copy)
    def project(i):
        there = lax.rem(chip + chips - i, chips)
        for d in range(1, n_tp):
            q = lax.rem(tp + d, n_tp)
            remote(
                hidden.at[there, q], hidden.at[there, q], h_send.at[there, q],
                h_recv.at[there, q], tp=q,
            ).wait_recv()
        total = None
        for q in range(n_tp):
            part = dot(hidden[there, q], down[q * ff : (q + 1) * ff, :])
            total = part if total is None else total + part
        result[there] = total.astype(jnp.bfloat16).reshape(pair, cap, columns)
        for c in range(pair):
            if i == 0 and c == 0:
                returned[ep] = result[there, lax.rem(ep, pair)]
                continue
            core = lax.rem(ep + c, pair) if i == 0 else c
            target = pair * there + core
            go(remote(
                result.at[there, core], returned.at[ep], r_send.at[target], r_recv.at[ep],
                ep=target,
            ))

    for copy in loads[2:]:
        copy.wait()
    for i in range(1, chips):
        expand(i)
        project(i - 1)
    for copy in mixes:
        copy.wait_recv()
    total = None
    for q in range(n_tp):
        part = dot(active[q], weight_ref[q * channels : (q + 1) * channels, :])
        total = part if total is None else total + part
    out_ref[...] = total.astype(out_ref.dtype)
    for copy in shares:
        copy.wait_recv()
    width = shared.shape[2]
    common = None
    for q in range(n_tp):
        part = dot(shared[q], sdown_ref[q * width : (q + 1) * width, :])
        common = part if common is None else common + part
    project(chips - 1)
    for source in others:
        remote(
            returned.at[source], returned.at[source], r_send.at[source], r_recv.at[source],
            ep=source,
        ).wait_recv()
    back = returned[...].reshape(n_ep * cap, columns)
    high, low = halves(gains[...])
    experts_ref[...] = (common + (dot(high, back) + dot(low, back))).astype(experts_ref.dtype)
    for copy in sends:
        copy.wait_send()


def shards(
    mixer_input,
    log_step,
    decay_shift,
    input_map,
    readout,
    mixer_weight,
    expert_input,
    norm_gain,
    routes,
    route_weight,
    expert_switch_matrix,
    up_weight,
    down_weight,
    shared_gate,
    shared_up,
    shared_down,
):
    n_ep, n_tp = lax.axis_size("ep"), lax.axis_size("tp")
    token_count, features = expert_input.shape
    top_count = routes.shape[1]
    cap = 2 * token_count * top_count // n_ep
    values = expert_input.astype(jnp.float32)
    normed = (
        values * lax.rsqrt(jnp.mean(values * values, axis=-1, keepdims=True) + 1e-06) * norm_gain
    ).astype(jnp.bfloat16)
    flat_routes = routes.reshape(-1)
    onehot = (flat_routes[:, None] == jnp.arange(n_ep, dtype=jnp.int32)[None, :]).astype(jnp.int32)
    before = jnp.sum((jnp.cumsum(onehot, axis=0) - onehot) * onehot, axis=1)
    slot = (flat_routes * cap + before).reshape(token_count, top_count)
    hit = slot[:, :, None] == jnp.arange(n_ep * cap, dtype=jnp.int32)[None, None, :]
    gains = jnp.sum(jnp.where(hit, route_weight[:, :, None], 0.0), axis=1)
    chosen = jnp.any(hit, axis=1).astype(jnp.bfloat16)
    outgoing = lax.dot_general(
        chosen, normed, (((0,), (0,)), ((), ())), preferred_element_type=jnp.float32
    ).astype(jnp.bfloat16).reshape(n_ep, cap, features)

    rows, channels = mixer_input.shape
    groups = log_step.shape[0]
    states, width = input_map.shape[2:]
    merged = groups * states
    _, cosine, sine, inject_re, inject_im = factors(log_step, states)
    table = jnp.stack([a.reshape(merged) for a in (cosine, sine, inject_re, inject_im)])
    f32, bf16 = jnp.float32, jnp.bfloat16
    pair = 2 if n_ep % 2 == 0 else 1
    chips = n_ep // pair
    ff = up_weight.shape[2]
    depth, columns = down_weight.shape[1:]
    vmem = pl.BlockSpec(memory_space=pltpu.VMEM)
    dma = pltpu.SemaphoreType.DMA
    return tuple(pl.pallas_call(
        functools.partial(fused_kernel, n_ep, n_tp, states),
        out_shape=(
            jax.ShapeDtypeStruct((rows, mixer_weight.shape[1]), bf16),
            jax.ShapeDtypeStruct((token_count, columns), bf16),
        ),
        in_specs=[vmem] * 13 + [pl.BlockSpec(memory_space=pl.ANY)] * 3,
        out_specs=(vmem, vmem),
        scratch_shapes=[
            pltpu.VMEM((rows, merged), f32),
            pltpu.VMEM((rows, merged), f32),
            pltpu.VMEM((rows, merged), f32),
            pltpu.VMEM((4, SUBLANES, merged), f32),
            pltpu.VMEM((n_ep, 4, merged), f32),
            pltpu.VMEM((n_tp, rows, channels), bf16),
            pltpu.VMEM((features, ff), bf16),
            pltpu.VMEM((features, ff), bf16),
            pltpu.VMEM((depth, columns), bf16),
            pltpu.VMEM((n_ep, cap, features), bf16),
            pltpu.VMEM((chips, n_tp, pair * cap, ff), bf16),
            pltpu.VMEM((chips, pair, cap, columns), bf16),
            pltpu.VMEM((n_ep, cap, columns), bf16),
            pltpu.VMEM((n_tp, token_count, shared_up.shape[1]), bf16),
            dma((n_ep,)), dma((n_ep,)), dma((n_tp,)), dma((n_tp,)),
            dma((n_ep,)), dma((n_ep,)), dma((chips, n_tp)), dma((chips, n_tp)),
            dma((n_ep,)), dma((n_ep,)), dma((n_tp,)), dma((n_tp,)), dma((3,)),
        ],
        compiler_params=pltpu.CompilerParams(
            collective_id=0, has_side_effects=True, vmem_limit_bytes=56 * 1024 * 1024
        ),
        name="fused",
    )(
        mixer_input,
        log_step.reshape(1, groups),
        decay_shift,
        input_map.reshape(2, merged, width),
        readout.reshape(2, channels, states),
        table,
        mixer_weight,
        outgoing,
        gains,
        normed,
        shared_gate,
        shared_up,
        shared_down,
        expert_switch_matrix,
        up_weight,
        down_weight,
    ))


def solution(mesh):
    placed = (
        P("ep", "tp"),
        P("tp"),
        P("ep", "tp"),
        P(None, "tp", None, None),
        P(None, "tp", None, None),
        P(None, "tp"),
        P("ep", None),
        P(),
        P("ep", None),
        P("ep", None),
        P("ep", None, "tp"),
        P("ep", None, "tp"),
        P("ep", None, "tp"),
        P(None, "tp"),
        P(None, "tp"),
        P(None, "tp"),
    )
    return jax.shard_map(
        shards,
        mesh=mesh,
        in_specs=placed,
        out_specs=(P("ep", "tp"), P("ep", "tp")),
        check_vma=False,
    )
```

profile of v0, /device:TPU:1, one launch (start us, length us, event | category | flops | bytes accessed | tf_op | source)
XLA Modules:
  0.0 109.1 jit_solution(12654188588584079122)
XLA Ops:
  0.6 1.2 %fusion = f32[128]{0:T(128)S(1)} fusion(bf16[128,2048]{1,0:T(8,128)(2,1)} %param.22), kind=kLoop, calls=%fused_computation.3 | loop fusion | flops 786304 | bytes 524800 | tf_op jit(solution)/shard_map/reduce_sum | solution.py:382
  1.9 0.7 fusion.7
  2.6 0.1 mul.225
  2.6 0.1 mul.226
  2.7 0.1 mul.241
  2.8 0.1 mul.230
  2.9 0.1 mul.233
  2.9 0.1 mul.234
  3.0 0.2 add_multiply_fusion
  3.2 0.6 pad_maximum_fusion.table_ref
  3.8 0.8 copy.37
  4.6 0.1 eq.42
  4.7 0.1 eq.38
  4.9 0.6 reduce-window.6
  5.5 0.2 slice_reduce_fusion
  5.7 0.1 fusion.5
  5.8 0.1 reduce_sum.30
  6.0 0.1 copy.39
  6.0 0.7 multiply_add_fusion.1
  6.7 0.1 fusion.3
  6.9 1.5 %copy.40.shift_ref = f32[256,16]{1,0:T(8,128)} copy(f32[256,16]{0,1:T(8,128)} %param.18) | data formatting | bytes 32768 | tf_op args[2]
  8.3 1.5 %select_reduce_fusion.gains = f32[128,512]{1,0:T(8,128)} fusion(f32[128,2]{0,1:T(2,128)} %param.25, s32[128,2]{0,1:T(2,128)S(1)} %multiply_add_fusion.1), kind=kLoop, calls=%fused_computation.6 | loop fusion | flops 327680 | bytes 264192 | tf_op jit(solution)/shard_map/reduce_sum | solution.py:389
  9.9 1.2 %fusion.2.normed = bf16[128,2048]{1,0:T(8,128)(2,1)S(1)} fusion(bf16[128,2048]{1,0:T(8,128)(2,1)} %param.22, f32[2048]{0:T(1024)} %param.23, f32[128]{0:T(128)S(1)} %add_rsqrt_fusion), kind=kLoop, calls=%fused_computation.5 | loop fusion | flops 1048576 | bytes 1057280 | tf_op jit(solution)/shard_map/convert_element_type | solution.py:383
  11.1 0.0 copy-start
  11.1 2.1 %copy.36 = bf16[2,16,64,16]{3,2,1,0:T(8,128)(2,1)} copy(bf16[2,16,64,16]{2,3,1,0:T(8,128)(2,1)} %param.19) | data formatting | bytes 131072 | tf_op args[3]
  13.2 2.1 %convolution_convert_fusion = bf16[512,2048]{1,0:T(8,128)(2,1)} fusion(pred[128,512]{1,0:T(8,128)(4,1)S(1)} %fusion.3, bf16[128,2048]{1,0:T(8,128)(2,1)S(1)} %fusion.2.normed), kind=kOutput, calls=%fused_computation | convolution fusion | flops 269484032 | bytes 2686976 | tf_op jit(solution)/shard_map/dot_general | solution.py:391
  15.3 0.0 copy-done
  15.3 90.5 %fused.1 = (bf16[256,512]{1,0:T(8,128)(2,1)}, bf16[128,512]{1,0:T(8,128)(2,1)}) custom-call(bf16[256,256]{1,0:T(8,128)(2,1)} %x_ref.1, f32[1,16]{1,0:T(1,128)} %bitcast.17, f32[256,16]{1,0:T(8,128)} %copy.40.shift_ref, bf16[2,1024,16]{2,1,0:T(8,128)(2,1)} %bitcast.15, f32[2,256,64]{2,1,0:T(8,128)} %bitcast.16, f32[4,1024]{1,0:T(4,128)} %pad_maximum_fusion.table_ref, ...), custom_call_target="tpu_custom_call" | custom-call | tf_op jit(solution)/shard_map/fused/pallas_call | solution.py:408
  105.8 1.7 %copy.43 = bf16[256,512]{1,0:T(8,128)(2,1)} copy(bf16[256,512]{1,0:T(8,128)(2,1)} %get-tuple-element.10) | data formatting | bytes 524288
  107.5 1.6 %copy.44 = bf16[128,512]{1,0:T(8,128)(2,1)} copy(bf16[128,512]{1,0:T(8,128)(2,1)} %get-tuple-element.11) | data formatting | bytes 262144
  (8 shorter events, 0.1 us)
Async XLA Ops:
  11.1 4.2 %copy-start = (bf16[128,2048]{1,0:T(8,128)(2,1)}, bf16[128,2048]{1,0:T(8,128)(2,1)S(1)}, u32[]{:S(2)}) copy-start(bf16[128,2048]{1,0:T(8,128)(2,1)S(1)} %fusion.2.normed) | copy-start | bytes 1572868
where the time goes:
time: 110 us; the launch traced here: 109 us
  Pallas kernels  90.5 us (82%)
  local copies, waits for them, and re-layouts  8.72 us (8%)
  other arithmetic  7.01 us (6%)
  matrix products  2.11 us (2%)
    pallas_call x1, Pallas kernels, shards(): pl.pallas_call(functools.partial(fused_kernel, n_ep, n_tp, states), out_s...  90.5 us
    unnamed x7, local copies, waits for them, and re-layouts  7.56 us

commit v1 on v0

v1 whole, which is shorter than its diff:
```python
import functools
import math

import jax
import jax.numpy as jnp
from jax import lax
from jax.experimental import pallas as pl
from jax.experimental.pallas import tpu as pltpu
from jax.sharding import PartitionSpec as P

MESH = pl.DeviceIdType.MESH
SUBLANES = 8
NT = (((1,), (1,)), ((), ()))
TN = (((0,), (0,)), ((), ()))


def times(ar, ai, br, bi):
    return ar * br - ai * bi, ar * bi + ai * br


def iota(shape, dim):
    return lax.broadcasted_iota(jnp.int32, shape, dim)


def spread(shape, period):
    return (iota(shape, 1) % period == iota(shape, 0)).astype(jnp.bfloat16)


def halves(a):
    high = a.astype(jnp.bfloat16)
    return high, (a - high.astype(jnp.float32)).astype(jnp.bfloat16)


def dot(a, b, dims=None):
    if dims is None:
        return jnp.dot(a, b, preferred_element_type=jnp.float32)
    return lax.dot_general(a, b, dims, preferred_element_type=jnp.float32)


def fill_table(rate_ref, table, states):
    groups = rate_ref.shape[1]
    merged = table.shape[1]
    same = iota((groups, groups), 0) == iota((groups, groups), 1)
    column = jnp.sum(jnp.where(same, rate_ref[...], 0.0), axis=1, keepdims=True)
    place = iota((groups, merged), 1) // states == iota((groups, merged), 0)
    wide = jnp.sum(jnp.where(place, column, 0.0), axis=0, keepdims=True)
    step_rate = jnp.exp(wide)
    frequency = jnp.pi * lax.rem(iota((1, merged), 1), states).astype(jnp.float32)
    angle = step_rate * frequency
    turn_cosine = jnp.cos(angle)
    turn_sine = jnp.sin(angle)
    base = jnp.exp(-0.5 * step_rate)
    starting_quadrature = base * turn_sine
    inverse = 1.0 / (0.25 + frequency * frequency)
    lowered = base * turn_cosine - 1.0
    table[0:1, :] = turn_cosine
    table[1:2, :] = turn_sine
    table[2:3, :] = (-0.5 * lowered + starting_quadrature * frequency) * inverse
    table[3:4, :] = (-0.5 * starting_quadrature - lowered * frequency) * inverse
    return column


def drive_into(x_ref, column, shift_ref, map_ref, table_ref, mag, push_re, push_im, states):
    rows, channels = x_ref.shape
    merged = mag.shape[1]
    groups = shift_ref.shape[0]
    width = channels // groups
    steps = rows // SUBLANES
    place = iota((rows, rows), 0)
    order = (iota((rows, rows), 1) == (place % SUBLANES) * steps + place // SUBLANES).astype(
        jnp.bfloat16
    )
    level = jnp.exp(-0.5 * jnp.exp(column) + shift_ref[...])
    high, middle = halves(level)
    low = ((level - high.astype(jnp.float32)) - middle.astype(jnp.float32)).astype(jnp.bfloat16)
    widen = (iota((groups, merged), 1) // states == iota((groups, merged), 0)).astype(jnp.bfloat16)
    total = None
    for piece in (high, middle, low):
        part = dot(dot(order, piece, NT).astype(jnp.bfloat16), widen)
        total = part if total is None else total + part
    mag[...] = total
    x = dot(order, x_ref[...]).astype(jnp.bfloat16)
    repeat = spread((states, merged), states)
    mine = iota((channels, merged), 1) // states == iota((channels, merged), 0) // width
    drives = []
    for c in range(2):
        wide = jnp.where(mine, dot(map_ref[c], repeat), 0.0).astype(jnp.bfloat16)
        drives.append(dot(x, wide))
    re, im = times(table_ref[2:3, :], table_ref[3:4, :], drives[0], drives[1])
    push_re[...] = re
    push_im[...] = im


def sweep(table_ref, mag, push_re, push_im, start_re, start_im, keep):
    rows, merged = mag.shape
    turn_re = jnp.broadcast_to(table_ref[0:1, :], (SUBLANES, merged))
    turn_im = jnp.broadcast_to(table_ref[1:2, :], (SUBLANES, merged))

    def one(j, carry):
        re, im, product = carry
        at = pl.ds(pl.multiple_of(j * SUBLANES, SUBLANES), SUBLANES)
        level = mag[at, :]
        next_re, next_im = times(turn_re, turn_im, re, im)
        next_re = level * next_re + push_re[at, :]
        next_im = level * next_im + push_im[at, :]
        if keep:
            push_re[at, :] = next_re
            push_im[at, :] = next_im
        else:
            product = product * level
        return next_re, next_im, product

    product = jnp.ones((SUBLANES, merged), jnp.float32)
    if keep:
        def pair(j, carry):
            return one(j, carry + (None,))[:2]
        return lax.fori_loop(0, rows // SUBLANES, pair, (start_re, start_im))
    return lax.fori_loop(0, rows // SUBLANES, one, (start_re, start_im, product))


def join(table_ref, ends_re, ends_im, product, pre, steps):
    merged = ends_re.shape[1]
    wr, wi = table_ref[0:1, :], table_ref[1:2, :]
    power = 1
    while power < steps:
        wr, wi = times(wr, wi, wr, wi)
        power *= 2
    cr = jnp.zeros((1, merged), jnp.float32)
    ci = cr
    ar = cr + 1.0
    ai = cr
    for s in range(SUBLANES):
        for i, v in enumerate((cr, ci, ar, ai)):
            pre[i, s : s + 1, :] = v
        level = product[s : s + 1]
        fr, fi = level * wr, level * wi
        tr, ti = times(fr, fi, cr, ci)
        cr, ci = tr + ends_re[s : s + 1], ti + ends_im[s : s + 1]
        ar, ai = times(fr, fi, ar, ai)
    return cr, ci, ar, ai


def read_states(readout_ref, push_re, push_im, states):
    rows, merged = push_re.shape
    channels = readout_ref.shape[1]
    width = channels * states // merged
    repeat = spread((states, merged), states)
    mine = iota((channels, merged), 1) // states == iota((channels, merged), 0) // width
    total = None
    for c, ref in enumerate((push_re, push_im)):
        high, low = halves(ref[...])
        back = readout_ref[c] if c == 0 else -readout_ref[c]
        wide_high, wide_low = (
            jnp.where(mine, dot(half, repeat), 0.0).astype(jnp.bfloat16) for half in halves(back)
        )
        part = dot(high, wide_high, NT) + (dot(low, wide_high, NT) + dot(high, wide_low, NT))
        total = part if total is None else total + part
    place = iota((rows, rows), 0)
    steps = rows // SUBLANES
    order = (iota((rows, rows), 1) == (place % steps) * SUBLANES + place // steps).astype(
        jnp.bfloat16
    )
    cube = total + 0.044715 * (total * total * total)
    active = (0.5 * total * (1.0 + jnp.tanh(0.7978845608028654 * cube))).astype(jnp.bfloat16)
    return dot(order, active).astype(jnp.bfloat16)


def remote(src, dst, send, recv, **target):
    return pltpu.make_async_remote_copy(
        src_ref=src, dst_ref=dst, send_sem=send, recv_sem=recv,
        device_id=target, device_id_type=MESH,
    )


def visits(chips):
    plan = []
    for chip in range(chips):
        units = []
        for d in range(1, chips):
            for j in range(2):
                together = False
                for there, onward in ((chip - d, chip + 1), (chip + d, chip - 1)):
                    if 0 <= there < chips:
                        onward = onward if 0 <= onward < chips else -1
                        units.append((2 * there + j, onward, int(together)))
                        together = True
        plan.append(units)
    return plan


def fused_kernel(
    n_ep, n_tp, states,
    routes_ref, gains_ref, rate_ref, gain_ref,
    input_hbm, x_hbm, shift_hbm, map_hbm, readout_hbm, weight_hbm,
    sgate_hbm, sup_hbm, sdown_hbm, gate_hbm, up_hbm, down_hbm,
    out_ref, experts_ref,
    tokens, x_ref, shift_ref, map_ref, readout_ref, weight_ref,
    sgate, sup, sdown, gate, up, down,
    table, mag, push_re, push_im, pre, summary, active,
    tok, named, picked, hidden, result, returned, shared, common, high, low,
    load, tok_recv, mate_send, own_send, on_send, n_send, n_recv,
    e_send, e_recv, a_send, a_recv, h_send, h_recv, r_send, r_recv, s_send, s_recv,
):
    ep = lax.axis_index("ep")
    tp = lax.axis_index("tp")
    rows, channels = x_ref.shape
    merged = mag.shape[1]
    half_rows, features = tok.shape[2:]
    count = 2 * half_rows
    cap = picked.shape[0]
    chips = n_ep // 2
    chip, core = ep // 2, lax.rem(ep, 2)
    mate = ep + 1 - 2 * core
    side = math.isqrt(n_tp)
    y, x = tp // side, lax.rem(tp, side)
    half = hidden.shape[4]

    barrier = pltpu.get_barrier_semaphore()
    for d in range(1, n_ep):
        pl.semaphore_signal(
            barrier, inc=1, device_id={"ep": lax.rem(ep + d, n_ep)}, device_id_type=MESH
        )
    for d in range(1, n_tp):
        pl.semaphore_signal(
            barrier, inc=1, device_id={"tp": lax.rem(tp + d, n_tp)}, device_id_type=MESH
        )
    pairs = (
        (input_hbm, tokens), (sgate_hbm, sgate), (sup_hbm, sup), (gate_hbm, gate), (up_hbm, up),
        (x_hbm, x_ref), (shift_hbm, shift_ref), (map_hbm, map_ref), (down_hbm, down),
        (readout_hbm, readout_ref), (weight_hbm, weight_ref), (sdown_hbm, sdown),
    )
    loads = [pltpu.make_async_copy(a, b, load.at[i]) for i, (a, b) in enumerate(pairs)]
    for copy in loads:
        copy.start()
    sends = []

    def go(copy):
        copy.start()
        sends.append(copy)

    def across(dy, dx):
        return lax.rem(y + dy, side) * side + lax.rem(x + dx, side)

    peers = {(dy, dx): across(dy, dx) for dy in range(side) for dx in range(side)}

    class Share:
        def __init__(self, at, send, recv):
            self.at, self.send, self.recv = at, send, recv

        def copy(self, source, h, dy, dx, to):
            return remote(
                self.at(source, h), self.at(source, h), self.send(h, dy, dx),
                self.recv(source, h), tp=to,
            )

        def start(self, h):
            for o in range(1, side):
                go(self.copy(tp, h, 0, o, peers[0, o]))
                go(self.copy(tp, h, o, 0, peers[o, 0]))

        def wait(self, source, h):
            self.copy(source, h, 0, 0, source).wait_recv()

        def forward(self):
            for o in range(1, side):
                self.wait(peers[0, o], 0)
                for d in range(1, side):
                    go(self.copy(peers[0, o], 0, d, o, peers[d, 0]))
                self.wait(peers[o, 0], 1)
                for d in range(1, side):
                    go(self.copy(peers[o, 0], 1, o, d, peers[0, d]))

        def near(self):
            for o in range(1, side):
                self.wait(peers[0, o], 1)
                self.wait(peers[o, 0], 0)

        def far(self):
            for dy in range(1, side):
                for dx in range(1, side):
                    for h in range(2):
                        self.wait(peers[dy, dx], h)

    def hidden_of(s):
        return Share(
            lambda q, h: hidden.at[s, q, h],
            lambda h, dy, dx: h_send.at[s, h, dy * side + dx],
            lambda q, h: h_recv.at[s, q, h],
        )

    shared_out = Share(
        lambda q, h: shared.at[q, h],
        lambda h, dy, dx: s_send.at[h, dy * side + dx],
        lambda q, h: s_recv.at[q, h],
    )
    active_out = Share(
        lambda q, h: active.at[q, h],
        lambda h, dy, dx: a_send.at[h, dy * side + dx],
        lambda q, h: a_recv.at[q, h],
    )

    loads[0].wait()
    block = 16
    scale = gain_ref[...]

    @pl.loop(0, half_rows // block)
    def _(i):
        at = pl.ds(pl.multiple_of(i * block, block), block)
        for h in range(2):
            values = tokens[h, at, :].astype(jnp.float32)
            level = lax.rsqrt(jnp.mean(values * values, axis=-1, keepdims=True) + 1e-06)
            tok[ep, h, at, :] = (values * level * scale).astype(jnp.bfloat16)

    named[ep] = routes_ref[...]
    pl.semaphore_wait(barrier, n_ep + n_tp - 2)

    def piece(s, h, send, target):
        return remote(tok.at[s, h], tok.at[s, h], send, tok_recv.at[s, h], ep=target)

    go(piece(ep, 1 - core, mate_send.at[ep, 1 - core], mate))
    go(piece(ep, core, mate_send.at[ep, core], mate))
    for d in range(1, n_ep):
        target = lax.rem(ep + d, n_ep)
        go(remote(routes_ref, named.at[ep], n_send.at[d], n_recv.at[ep], ep=target))
    ends = ((chip > 0, lax.rem(ep + n_ep - 2, n_ep)), (chip < chips - 1, lax.rem(ep + 2, n_ep)))

    def own(j, d):
        return piece(2 * chip + j, core, own_send.at[d, j], ends[d][1])

    for j in range(2):
        @pl.when(core != j)
        def _():
            piece(2 * chip + j, core, mate_send.at[mate, core], mate).wait_recv()

        for d in range(2):
            @pl.when(ends[d][0])
            def _():
                own(j, d).start()

    def shared_hidden():
        for copy in loads[1:3]:
            copy.wait()
        a = tok[ep].reshape(count, features)
        v = dot(a, sgate[...])
        shared[tp] = (v / (1.0 + jnp.exp(-v)) * dot(a, sup[...])).astype(jnp.bfloat16).reshape(
            shared.shape[1:]
        )
        for h in range(2):
            shared_out.start(h)

    later = (iota((count, count), 0) <= iota((count, count), 1)).astype(jnp.bfloat16)
    slots = iota((cap, count), 0).astype(jnp.float32)

    def member(names, expert):
        return jnp.logical_or(names[0:1] == expert, names[1:2] == expert)

    def seats(mine):
        ones = jnp.where(mine, 1.0, 0.0)
        ranks = dot(ones.astype(jnp.bfloat16), later)
        return jnp.where(mine, ranks - 1.0, -1.0)

    tile = min(half, 256)

    def process(s):
        names = named[s]
        place = seats(jnp.broadcast_to(member(names, ep), (SUBLANES, count)))
        chosen = (slots == place[0:1]).astype(jnp.bfloat16)
        picked[...] = dot(chosen, tok[s].reshape(count, features)).astype(jnp.bfloat16)
        share = hidden_of(s)
        for h in range(2):
            @pl.loop(0, half // tile)
            def _(n):
                inner = pl.ds(pl.multiple_of(n * tile, tile), tile)
                at = pl.ds(pl.multiple_of(h * half + n * tile, tile), tile)
                a = picked[...]
                v = dot(a, gate[:, at])
                hidden[s, tp, h, :, inner] = (
                    v / (1.0 + jnp.exp(-v)) * dot(a, up[:, at])
                ).astype(jnp.bfloat16)

            share.start(h)

    def back(s):
        return remote(result.at[s], returned.at[ep], r_send.at[s], r_recv.at[ep], ep=s)

    def project(s, away=True):
        share = hidden_of(s)

        def part(q):
            return dot(hidden[s, q, 0], down[q, 0]) + dot(hidden[s, q, 1], down[q, 1])

        share.near()
        total = part(tp)
        for o in range(1, side):
            total = total + part(peers[0, o])
            total = total + part(peers[o, 0])
        share.far()
        for dy in range(1, side):
            for dx in range(1, side):
                total = total + part(peers[dy, dx])
        if away:
            result[s] = total.astype(jnp.bfloat16)
            go(back(s))
        else:
            returned[s] = total.astype(jnp.bfloat16)

    def scan_block():
        for copy in loads[5:8]:
            copy.wait()
        column = fill_table(rate_ref, table, states)
        drive_into(x_ref, column, shift_ref, map_ref, table, mag, push_re, push_im, states)
        zero = jnp.zeros((SUBLANES, merged), jnp.float32)
        ends_re, ends_im, product = sweep(table, mag, push_re, push_im, zero, zero, False)
        end = join(table, ends_re, ends_im, product, pre, rows // SUBLANES)
        for i, v in enumerate(end):
            summary[ep, i : i + 1, :] = v
        for d in range(1, n_ep):
            go(remote(
                summary.at[ep], summary.at[ep], e_send.at[d], e_recv.at[ep],
                ep=lax.rem(ep + d, n_ep),
            ))

    def gain_blocks():
        names = routes_ref[...]
        level = gains_ref[...]
        for e in range(n_ep):
            place = seats(jnp.broadcast_to(member(names, e), (SUBLANES, count)))
            weight = jnp.where(names[0:1] == e, level[0:1], 0.0) + jnp.where(
                names[1:2] == e, level[1:2], 0.0
            )
            wide = jnp.where(slots == place[0:1], weight, 0.0)
            top, rest = halves(wide)
            high[e * cap : (e + 1) * cap, :] = top
            low[e * cap : (e + 1) * cap, :] = rest

    def scan_states():
        for d in range(1, n_ep):
            e = lax.rem(ep + d, n_ep)
            remote(
                summary.at[e], summary.at[e], e_send.at[d], e_recv.at[e], ep=e
            ).wait_recv()

        def fold(e, carry):
            part = summary[e]
            re, im = times(part[2:3], part[3:4], carry[0], carry[1])
            return re + part[0:1], im + part[1:2]

        nothing = jnp.zeros((1, merged), jnp.float32)
        in_re, in_im = lax.fori_loop(0, ep, fold, (nothing, nothing))
        add_re, add_im = times(pre[2], pre[3], in_re, in_im)
        sweep(table, mag, push_re, push_im, pre[0] + add_re, pre[1] + add_im, True)
        loads[9].wait()
        active[tp] = read_states(readout_ref, push_re, push_im, states).reshape(active.shape[1:])
        for h in range(2):
            active_out.start(h)

    def mix():
        active_out.near()
        active_out.far()
        loads[10].wait()
        total = None
        for q in range(n_tp):
            a = active[q].reshape(rows, channels)
            part = dot(a, weight_ref[q * channels : (q + 1) * channels, :])
            total = part if total is None else total + part
        out_ref[...] = total.astype(out_ref.dtype)
        shared_out.near()
        shared_out.far()
        loads[11].wait()
        width = shared.shape[3]
        total = None
        for q in range(n_tp):
            a = shared[q].reshape(count, width)
            part = dot(a, sdown[q * width : (q + 1) * width, :])
            total = part if total is None else total + part
        common[...] = total

    plan = visits(chips)
    last = len(plan[0]) - 1

    def here(u, field):
        value = jnp.int32(plan[0][u][field])
        for k in range(1, chips):
            value = jnp.where(chip == k, jnp.int32(plan[k][u][field]), value)
        return value

    source = [here(u, 0) for u in range(last + 1)]
    onward = [here(u, 1) for u in range(last + 1)]
    paired = [here(u, 2) for u in range(last + 1)]

    def along(u):
        target = 2 * jnp.maximum(onward[u], 0) + core
        return piece(source[u], core, on_send.at[source[u]], target)

    def aside(u):
        return piece(source[u], core, mate_send.at[source[u], core], mate)

    def pass_on(u):
        aside(u).wait_recv()

        @pl.when(onward[u] >= 0)
        def _():
            along(u).start()

        aside(u).start()

    shared_hidden()
    for copy in loads[3:5]:
        copy.wait()
    process(ep)
    piece(mate, 1 - core, mate_send.at[mate, 1 - core], mate).wait_recv()

    def names_of(s):
        remote(routes_ref, named.at[s], n_send.at[0], n_recv.at[s], ep=s).wait_recv()

    names_of(mate)
    process(mate)
    scan_block()
    gain_blocks()
    shared_out.forward()
    order = [ep, mate] + source
    for u in range(last + 1):
        @pl.when(paired[u] == 0)
        def _():
            pass_on(u)

        if u < last:
            @pl.when(paired[u + 1] == 1)
            def _():
                pass_on(u + 1)

        if u == 0:
            hidden_of(ep).forward()
        hidden_of(order[u + 1]).forward()
        s = source[u]
        piece(s, 1 - core, mate_send.at[s, 1 - core], mate).wait_recv()
        names_of(s)
        process(s)
        if u == 0:
            loads[8].wait()
        project(order[u], away=u > 0)
        if u == min(2, last):
            scan_states()
        if u == min(3, last):
            active_out.forward()
        if u == min(4, last):
            mix()
    hidden_of(order[-1]).forward()
    project(order[-2])
    project(order[-1])
    for d in range(1, n_ep):
        e = lax.rem(ep + d, n_ep)
        remote(returned.at[e], returned.at[e], r_send.at[e], r_recv.at[e], ep=e).wait_recv()
    back_rows = returned[...].reshape(n_ep * cap, returned.shape[2])
    routed = dot(high[...], back_rows, TN) + dot(low[...], back_rows, TN)
    experts_ref[...] = (common[...] + routed).astype(experts_ref.dtype)
    for copy in sends:
        copy.wait_send()
    for j in range(2):
        for d in range(2):
            @pl.when(ends[d][0])
            def _():
                own(j, d).wait_send()
    for u in range(last + 1):
        aside(u).wait_send()

        @pl.when(onward[u] >= 0)
        def _():
            along(u).wait_send()


def shards(
    mixer_input,
    log_step,
    decay_shift,
    input_map,
    readout,
    mixer_weight,
    expert_input,
    norm_gain,
    routes,
    route_weight,
    expert_switch_matrix,
    up_weight,
    down_weight,
    shared_gate,
    shared_up,
    shared_down,
):
    n_ep, n_tp = lax.axis_size("ep"), lax.axis_size("tp")
    count, features = expert_input.shape
    cap = 2 * count * routes.shape[1] // n_ep
    rows, channels = mixer_input.shape
    groups = log_step.shape[0]
    states, width = input_map.shape[2:]
    merged = groups * states
    f32, bf16 = jnp.float32, jnp.bfloat16
    ff = up_weight.shape[2]
    depth, columns = down_weight.shape[1:]
    shared_ff = shared_up.shape[1]
    vmem = pl.BlockSpec(memory_space=pltpu.VMEM)
    anywhere = pl.BlockSpec(memory_space=pl.ANY)
    dma = pltpu.SemaphoreType.DMA
    operands = (
        expert_input.reshape(2, count // 2, features),
        mixer_input,
        decay_shift.T,
        input_map.swapaxes(2, 3).reshape(2, channels, states),
        readout.reshape(2, channels, states),
        mixer_weight,
        shared_gate,
        shared_up,
        shared_down,
        expert_switch_matrix.reshape(features, ff),
        up_weight.reshape(features, ff),
        down_weight.reshape(n_tp, 2, ff // 2, columns),
    )
    return tuple(pl.pallas_call(
        functools.partial(fused_kernel, n_ep, n_tp, states),
        out_shape=(
            jax.ShapeDtypeStruct((rows, mixer_weight.shape[1]), bf16),
            jax.ShapeDtypeStruct((count, columns), bf16),
        ),
        in_specs=[vmem] * 4 + [anywhere] * len(operands),
        out_specs=(vmem, vmem),
        scratch_shapes=[pltpu.VMEM(a.shape, a.dtype) for a in operands] + [
            pltpu.VMEM((4, merged), f32),
            pltpu.VMEM((rows, merged), f32),
            pltpu.VMEM((rows, merged), f32),
            pltpu.VMEM((rows, merged), f32),
            pltpu.VMEM((4, SUBLANES, merged), f32),
            pltpu.VMEM((n_ep, 4, merged), f32),
            pltpu.VMEM((n_tp, 2, rows // 2, channels), bf16),
            pltpu.VMEM((n_ep, 2, count // 2, features), bf16),
            pltpu.VMEM((n_ep, 2, count), jnp.int32),
            pltpu.VMEM((cap, features), bf16),
            pltpu.VMEM((n_ep, n_tp, 2, cap, ff // 2), bf16),
            pltpu.VMEM((n_ep, cap, columns), bf16),
            pltpu.VMEM((n_ep, cap, columns), bf16),
            pltpu.VMEM((n_tp, 2, count // 2, shared_ff), bf16),
            pltpu.VMEM((count, columns), f32),
            pltpu.VMEM((n_ep * cap, count), bf16),
            pltpu.VMEM((n_ep * cap, count), bf16),
            dma((len(operands),)), dma((n_ep, 2)), dma((n_ep, 2)), dma((2, 2)),
            dma((n_ep,)), dma((n_ep,)), dma((n_ep,)), dma((n_ep,)), dma((n_ep,)),
            dma((2, n_tp)), dma((n_tp, 2)), dma((n_ep, 2, n_tp)), dma((n_ep, n_tp, 2)),
            dma((n_ep,)), dma((n_ep,)), dma((2, n_tp)), dma((n_tp, 2)),
        ],
        compiler_params=pltpu.CompilerParams(
            collective_id=0, has_side_effects=True, vmem_limit_bytes=56 * 1024 * 1024
        ),
        name="fused",
    )(
        routes.T, route_weight.T, log_step.reshape(1, groups), norm_gain.reshape(1, features),
        *operands,
    ))


def solution(mesh):
    placed = (
        P("ep", "tp"),
        P("tp"),
        P("ep", "tp"),
        P(None, "tp", None, None),
        P(None, "tp", None, None),
        P(None, "tp"),
        P("ep", None),
        P(),
        P("ep", None),
        P("ep", None),
        P("ep", None, "tp"),
        P("ep", None, "tp"),
        P("ep", None, "tp"),
        P(None, "tp"),
        P(None, "tp"),
        P(None, "tp"),
    )
    return jax.shard_map(
        shards,
        mesh=mesh,
        in_specs=placed,
        out_specs=(P("ep", "tp"), P("ep", "tp")),
        check_vma=False,
    )
```

time: 110 us -> 76.8 us (0.70)
  Pallas kernels: 90.5 us -> 72.7 us
  other arithmetic: 7.01 us -> 0 us
  local copies, waits for them, and re-layouts: 8.72 us -> 3.24 us
  matrix products: 2.11 us -> 0 us
    pallas_call x1, Pallas kernels: 90.5 us -> 72.7 us  [shards(): pl.pallas_call(functools.partial(fused_kernel, n_ep, n_tp, states), out_s...]
    unnamed x7 -> x2, local copies, waits for them, and re-layouts: 7.56 us -> 3.24 us
    reduce_sum x3 -> x0, other arithmetic: 2.86 us -> none  [the longest x1 1.54 us: shards(): gains = jnp.sum(jnp.where(hit, route_weight[:, :, None], 0.0), axis=1)]
    dot_general x1 -> x0, matrix products: 2.11 us -> none  [shards(): lax.dot_general(chosen, normed, (((0,), (0,)), ((), ())), preferred_eleme...]
    another operation x3 -> x0, other arithmetic: 1.24 us -> none
    convert_element_type x2 -> x0, other arithmetic: 1.24 us -> none  [the longest x1 1.23 us: shards(): normed = (values * lax.rsqrt(jnp.mean(values * values, axis=-1, keepdims=...]
where the time goes in v1:
time: 76.8 us; the launch traced here: 76.6 us
  Pallas kernels  72.7 us (95%)
  local copies, waits for them, and re-layouts  3.24 us (4%)
    pallas_call x1, Pallas kernels, shards(): pl.pallas_call(functools.partial(fused_kernel, n_ep, n_tp, states), out_s...  72.7 us
    unnamed x2, local copies, waits for them, and re-layouts  3.24 us

profile of v1, /device:TPU:1, one launch (start us, length us, event | category | flops | bytes accessed | tf_op | source)
XLA Modules:
  0.0 76.6 jit_solution(14408678829221459166)
XLA Ops:
  0.6 72.7 %fused.1 = (bf16[256,512]{1,0:T(8,128)(2,1)}, bf16[128,512]{1,0:T(8,128)(2,1)}) custom-call(s32[2,128]{1,0:T(2,128)} %bitcast.21, f32[2,128]{1,0:T(2,128)} %bitcast.22, f32[1,16]{1,0:T(1,128)} %bitcast.23, f32[1,2048]{1,0:T(1,128)} %bitcast.20, bf16[2,64,2048]{2,1,0:T(8,128)(2,1)} %bitcast.16, bf16[256,256]{1,0:T(8,128)(2,1)} %x_hbm.1, f32[16,256]{1,0:T(8,128)} %bitcast.19, ...), custom_call_target="tpu_custom_call" | custom-call | tf_op jit(solution)/shard_map/fused/pallas_call | solution.py:618
  73.3 1.7 %copy.20 = bf16[256,512]{1,0:T(8,128)(2,1)} copy(bf16[256,512]{1,0:T(8,128)(2,1)} %get-tuple-element.4) | data formatting | bytes 524288
  75.0 1.6 %copy.21 = bf16[128,512]{1,0:T(8,128)(2,1)} copy(bf16[128,512]{1,0:T(8,128)(2,1)} %get-tuple-element.5) | data formatting | bytes 262144

commit v2 on v1

--- a/solution.py
+++ b/solution.py
@@ -175,15 +175,19 @@
 def visits(chips):
     plan = []
     for chip in range(chips):
-        units = []
+        end = chip in (0, chips - 1)
+        found = []
         for d in range(1, chips):
             for j in range(2):
-                together = False
                 for there, onward in ((chip - d, chip + 1), (chip + d, chip - 1)):
                     if 0 <= there < chips:
                         onward = onward if 0 <= onward < chips else -1
-                        units.append((2 * there + j, onward, int(together)))
-                        together = True
+                        found.append((2 * there + j, onward, 2 * d + j))
+        units = []
+        for u, (source, onward, arrival) in enumerate(found):
+            together = max(v for v in range(len(found)) if found[v][2] == arrival)
+            step = 2 * u if end else max(0, 2 * together - 3)
+            units.append((source, onward, step, int(end and u > 1)))
         plan.append(units)
     return plan
 
@@ -197,8 +201,8 @@
     tokens, x_ref, shift_ref, map_ref, readout_ref, weight_ref,
     sgate, sup, sdown, gate, up, down,
     table, mag, push_re, push_im, pre, summary, active,
-    tok, named, picked, hidden, result, returned, shared, common, high, low,
-    load, tok_recv, mate_send, own_send, on_send, n_send, n_recv,
+    tok, named, picked, hidden, result, returned, shared, common, high, low, out_v, experts_v,
+    load, store, tok_recv, mate_send, own_send, on_send, n_send, n_recv,
     e_send, e_recv, a_send, a_recv, h_send, h_recv, r_send, r_recv, s_send, s_recv,
 ):
     ep = lax.axis_index("ep")
@@ -207,7 +211,7 @@
     merged = mag.shape[1]
     half_rows, features = tok.shape[2:]
     count = 2 * half_rows
-    cap = picked.shape[0]
+    cap = picked.shape[0] // 2
     chips = n_ep // 2
     chip, core = ep // 2, lax.rem(ep, 2)
     mate = ep + 1 - 2 * core
@@ -232,72 +236,51 @@
     loads = [pltpu.make_async_copy(a, b, load.at[i]) for i, (a, b) in enumerate(pairs)]
     for copy in loads:
         copy.start()
-    sends = []
-
-    def go(copy):
-        copy.start()
-        sends.append(copy)
-
+    store_out = pltpu.make_async_copy(out_v, out_ref, store.at[0])
+    store_experts = pltpu.make_async_copy(experts_v, experts_ref, store.at[1])
     def across(dy, dx):
         return lax.rem(y + dy, side) * side + lax.rem(x + dx, side)
 
     peers = {(dy, dx): across(dy, dx) for dy in range(side) for dx in range(side)}
 
     class Share:
-        def __init__(self, at, send, recv):
-            self.at, self.send, self.recv = at, send, recv
-
-        def copy(self, source, h, dy, dx, to):
-            return remote(
-                self.at(source, h), self.at(source, h), self.send(h, dy, dx),
-                self.recv(source, h), tp=to,
-            )
+        def __init__(self, buffer, send, recv):
+            self.buffer, self.send, self.recv = buffer, send, recv
+
+        def copy(self, source, h, to, k):
+            at = self.buffer.at[source, h]
+            return remote(at, at, self.send, self.recv.at[k], tp=to)
 
         def start(self, h):
             for o in range(1, side):
-                go(self.copy(tp, h, 0, o, peers[0, o]))
-                go(self.copy(tp, h, o, 0, peers[o, 0]))
-
-        def wait(self, source, h):
-            self.copy(source, h, 0, 0, source).wait_recv()
+                self.copy(tp, h, peers[0, o], 0 if h == 0 else 2).start()
+                self.copy(tp, h, peers[o, 0], 1 if h == 1 else 2).start()
+
+        def wait(self, at, k):
+            remote(at, at, self.send, self.recv.at[k], tp=peers[0, 1]).wait_recv()
 
         def forward(self):
-            for o in range(1, side):
-                self.wait(peers[0, o], 0)
-                for d in range(1, side):
-                    go(self.copy(peers[0, o], 0, d, o, peers[d, 0]))
-                self.wait(peers[o, 0], 1)
-                for d in range(1, side):
-                    go(self.copy(peers[o, 0], 1, o, d, peers[0, d]))
+            for h in range(2):
+                self.wait(self.buffer.at[pl.ds(0, side - 1), h], h)
+                for o in range(1, side):
+                    for d in range(1, side):
+                        source, to = ((0, o), (d, 0)) if h == 0 else ((o, 0), (0, d))
+                        self.copy(peers[source], h, peers[to], 3).start()
 
         def near(self):
-            for o in range(1, side):
-                self.wait(peers[0, o], 1)
-                self.wait(peers[o, 0], 0)
+            self.wait(self.buffer.at[pl.ds(0, side - 1)], 2)
 
         def far(self):
-            for dy in range(1, side):
-                for dx in range(1, side):
-                    for h in range(2):
-                        self.wait(peers[dy, dx], h)
+            self.wait(self.buffer.at[pl.ds(0, (side - 1) ** 2)], 3)
+
+        def drain(self, at):
+            remote(at, at, self.send, self.recv.at[0], tp=peers[0, 1]).wait_send()
 
     def hidden_of(s):
-        return Share(
-            lambda q, h: hidden.at[s, q, h],
-            lambda h, dy, dx: h_send.at[s, h, dy * side + dx],
-            lambda q, h: h_recv.at[s, q, h],
-        )
-
-    shared_out = Share(
-        lambda q, h: shared.at[q, h],
-        lambda h, dy, dx: s_send.at[h, dy * side + dx],
-        lambda q, h: s_recv.at[q, h],
-    )
-    active_out = Share(
-        lambda q, h: active.at[q, h],
-        lambda h, dy, dx: a_send.at[h, dy * side + dx],
-        lambda q, h: a_recv.at[q, h],
-    )
+        return Share(hidden.at[s], h_send.at[0], h_recv.at[s])
+
+    shared_out = Share(shared, s_send.at[0], s_recv)
+    active_out = Share(active, a_send.at[0], a_recv)
 
     loads[0].wait()
     block = 16
@@ -317,20 +300,23 @@
     def piece(s, h, send, target):
         return remote(tok.at[s, h], tok.at[s, h], send, tok_recv.at[s, h], ep=target)
 
-    go(piece(ep, 1 - core, mate_send.at[ep, 1 - core], mate))
-    go(piece(ep, core, mate_send.at[ep, core], mate))
-    for d in range(1, n_ep):
-        target = lax.rem(ep + d, n_ep)
-        go(remote(routes_ref, named.at[ep], n_send.at[d], n_recv.at[ep], ep=target))
+    piece(ep, 1 - core, mate_send.at[0], mate).start()
+    piece(ep, core, mate_send.at[0], mate).start()
+    remote(routes_ref, named.at[ep], n_send.at[0], n_recv.at[0], ep=mate).start()
+    strangers = [
+        2 * lax.rem(chip + d, chips) + c for d in range(1, chips) for c in range(2)
+    ]
+    for target in strangers:
+        remote(routes_ref, named.at[ep], n_send.at[0], n_recv.at[1], ep=target).start()
     ends = ((chip > 0, lax.rem(ep + n_ep - 2, n_ep)), (chip < chips - 1, lax.rem(ep + 2, n_ep)))
 
     def own(j, d):
-        return piece(2 * chip + j, core, own_send.at[d, j], ends[d][1])
+        return piece(2 * chip + j, core, own_send.at[d], ends[d][1])
 
     for j in range(2):
         @pl.when(core != j)
         def _():
-            piece(2 * chip + j, core, mate_send.at[mate, core], mate).wait_recv()
+            piece(2 * chip + j, core, mate_send.at[0], mate).wait_recv()
 
         for d in range(2):
             @pl.when(ends[d][0])
@@ -361,48 +347,60 @@
 
     tile = min(half, 256)
 
-    def process(s):
-        names = named[s]
-        place = seats(jnp.broadcast_to(member(names, ep), (SUBLANES, count)))
-        chosen = (slots == place[0:1]).astype(jnp.bfloat16)
-        picked[...] = dot(chosen, tok[s].reshape(count, features)).astype(jnp.bfloat16)
-        share = hidden_of(s)
+    def process(*group):
+        for i, s in enumerate(group):
+            names = named[s]
+            place = seats(jnp.broadcast_to(member(names, ep), (SUBLANES, count)))
+            chosen = (slots == place[0:1]).astype(jnp.bfloat16)
+            picked[i * cap : (i + 1) * cap, :] = dot(
+                chosen, tok[s].reshape(count, features)
+            ).astype(jnp.bfloat16)
         for h in range(2):
             @pl.loop(0, half // tile)
             def _(n):
                 inner = pl.ds(pl.multiple_of(n * tile, tile), tile)
                 at = pl.ds(pl.multiple_of(h * half + n * tile, tile), tile)
-                a = picked[...]
+                a = picked[: len(group) * cap, :]
                 v = dot(a, gate[:, at])
-                hidden[s, tp, h, :, inner] = (
-                    v / (1.0 + jnp.exp(-v)) * dot(a, up[:, at])
-                ).astype(jnp.bfloat16)
-
-            share.start(h)
+                v = (v / (1.0 + jnp.exp(-v)) * dot(a, up[:, at])).astype(jnp.bfloat16)
+                for i, s in enumerate(group):
+                    hidden[s, tp, h, :, inner] = v[i * cap : (i + 1) * cap]
+
+            for s in group:
+                hidden_of(s).start(h)
 
     def back(s):
-        return remote(result.at[s], returned.at[ep], r_send.at[s], r_recv.at[ep], ep=s)
-
-    def project(s, away=True):
-        share = hidden_of(s)
-
+        return remote(result.at[s], returned.at[ep], r_send.at[0], r_recv.at[0], ep=s)
+
+    def project(*group, before=None):
         def part(q):
-            return dot(hidden[s, q, 0], down[q, 0]) + dot(hidden[s, q, 1], down[q, 1])
-
-        share.near()
+            total = None
+            for h in range(2):
+                a = jnp.concatenate([hidden[s, q, h] for s in group], axis=0)
+                one = dot(a, down[q, h])
+                total = one if total is None else total + one
+            return total
+
         total = part(tp)
+        if before is not None:
+            before()
+        for s in group:
+            hidden_of(s).near()
         for o in range(1, side):
             total = total + part(peers[0, o])
             total = total + part(peers[o, 0])
-        share.far()
+        for s in group:
+            hidden_of(s).far()
         for dy in range(1, side):
             for dx in range(1, side):
                 total = total + part(peers[dy, dx])
-        if away:
-            result[s] = total.astype(jnp.bfloat16)
-            go(back(s))
+        for i, s in enumerate(group):
+            result[s] = total[i * cap : (i + 1) * cap].astype(jnp.bfloat16)
+        if len(group) == 2:
+            returned[ep] = result[ep]
+            back(mate).start()
         else:
-            returned[s] = total.astype(jnp.bfloat16)
+            back(group[0]).start()
 
     def scan_block():
         for copy in loads[5:8]:
@@ -414,11 +412,10 @@
         end = join(table, ends_re, ends_im, product, pre, rows // SUBLANES)
         for i, v in enumerate(end):
             summary[ep, i : i + 1, :] = v
-        for d in range(1, n_ep):
-            go(remote(
-                summary.at[ep], summary.at[ep], e_send.at[d], e_recv.at[ep],
-                ep=lax.rem(ep + d, n_ep),
-            ))
+        for target in strangers + [mate]:
+            remote(
+                summary.at[ep], summary.at[ep], e_send.at[0], e_recv.at[0], ep=target
+            ).start()
 
     def gain_blocks():
         names = routes_ref[...]
@@ -434,11 +431,8 @@
             low[e * cap : (e + 1) * cap, :] = rest
 
     def scan_states():
-        for d in range(1, n_ep):
-            e = lax.rem(ep + d, n_ep)
-            remote(
-                summary.at[e], summary.at[e], e_send.at[d], e_recv.at[e], ep=e
-            ).wait_recv()
+        rest = summary.at[pl.ds(0, n_ep - 1)]
+        remote(rest, rest, e_send.at[0], e_recv.at[0], ep=mate).wait_recv()
 
         def fold(e, carry):
             part = summary[e]
@@ -463,7 +457,8 @@
             a = active[q].reshape(rows, channels)
             part = dot(a, weight_ref[q * channels : (q + 1) * channels, :])
             total = part if total is None else total + part
-        out_ref[...] = total.astype(out_ref.dtype)
+        out_v[...] = total.astype(out_v.dtype)
+        store_out.start()
         shared_out.near()
         shared_out.far()
         loads[11].wait()
@@ -486,14 +481,15 @@
 
     source = [here(u, 0) for u in range(last + 1)]
     onward = [here(u, 1) for u in range(last + 1)]
-    paired = [here(u, 2) for u in range(last + 1)]
+    steps = [here(u, 2) for u in range(last + 1)]
+    early = [here(u, 3) for u in range(last + 1)]
 
     def along(u):
         target = 2 * jnp.maximum(onward[u], 0) + core
-        return piece(source[u], core, on_send.at[source[u]], target)
+        return piece(source[u], core, on_send.at[0], target)
 
     def aside(u):
-        return piece(source[u], core, mate_send.at[source[u], core], mate)
+        return piece(source[u], core, mate_send.at[0], mate)
 
     def pass_on(u):
         aside(u).wait_recv()
@@ -504,69 +500,89 @@
 
         aside(u).start()
 
+    def ready(s):
+        piece(s, 1 - core, mate_send.at[0], mate).wait_recv()
+
+    groups = [(2 * chip, 2 * chip + 1)] + [(s,) for s in source]
+
+    def forward(group):
+        for s in group:
+            hidden_of(s).forward()
+
     shared_hidden()
     for copy in loads[3:5]:
         copy.wait()
-    process(ep)
-    piece(mate, 1 - core, mate_send.at[mate, 1 - core], mate).wait_recv()
-
-    def names_of(s):
-        remote(routes_ref, named.at[s], n_send.at[0], n_recv.at[s], ep=s).wait_recv()
-
-    names_of(mate)
-    process(mate)
+    ready(mate)
+    remote(routes_ref, named.at[mate], n_send.at[0], n_recv.at[0], ep=mate).wait_recv()
+    process(*groups[0])
     scan_block()
     gain_blocks()
     shared_out.forward()
-    order = [ep, mate] + source
+    rest = named.at[pl.ds(0, n_ep - 2)]
+    remote(rest, rest, n_send.at[0], n_recv.at[1], ep=mate).wait_recv()
+
+    def arrivals(step):
+        for v in range(last + 1):
+            if any(units[v][2] == step for units in plan):
+                @pl.when(steps[v] == step)
+                def _():
+                    pass_on(v)
+
     for u in range(last + 1):
-        @pl.when(paired[u] == 0)
+        arrivals(2 * u)
+
+        @pl.when(early[u] == 1)
         def _():
-            pass_on(u)
-
-        if u < last:
-            @pl.when(paired[u + 1] == 1)
-            def _():
-                pass_on(u + 1)
-
-        if u == 0:
-            hidden_of(ep).forward()
-        hidden_of(order[u + 1]).forward()
-        s = source[u]
-        piece(s, 1 - core, mate_send.at[s, 1 - core], mate).wait_recv()
-        names_of(s)
-        process(s)
-        if u == 0:
+            forward(groups[u])
+
+        ready(source[u])
+        process(source[u])
+        arrivals(2 * u + 1)
+
+        @pl.when(early[u] == 0)
+        def _():
+            forward(groups[u])
+
+        if u == 1:
             loads[8].wait()
-        project(order[u], away=u > 0)
+        if u > 0:
+            project(*groups[u - 1])
         if u == min(2, last):
             scan_states()
         if u == min(3, last):
             active_out.forward()
         if u == min(4, last):
             mix()
-    hidden_of(order[-1]).forward()
-    project(order[-2])
-    project(order[-1])
-    for d in range(1, n_ep):
-        e = lax.rem(ep + d, n_ep)
-        remote(returned.at[e], returned.at[e], r_send.at[e], r_recv.at[e], ep=e).wait_recv()
+    project(*groups[last])
+    project(*groups[last + 1], before=functools.partial(forward, groups[last + 1]))
+    rest = returned.at[pl.ds(0, n_ep - 1)]
+    remote(rest, rest, r_send.at[0], r_recv.at[0], ep=mate).wait_recv()
     back_rows = returned[...].reshape(n_ep * cap, returned.shape[2])
     routed = dot(high[...], back_rows, TN) + dot(low[...], back_rows, TN)
-    experts_ref[...] = (common[...] + routed).astype(experts_ref.dtype)
-    for copy in sends:
-        copy.wait_send()
-    for j in range(2):
-        for d in range(2):
-            @pl.when(ends[d][0])
-            def _():
-                own(j, d).wait_send()
-    for u in range(last + 1):
-        aside(u).wait_send()
-
-        @pl.when(onward[u] >= 0)
+    experts_v[...] = (common[...] + routed).astype(experts_v.dtype)
+    store_experts.start()
+    shared_out.drain(shared.at[pl.ds(0, n_tp - 1)])
+    active_out.drain(active.at[pl.ds(0, n_tp - 1)])
+    hidden_of(ep).drain(hidden.at[:, pl.ds(0, n_tp - 1)])
+
+    def drain(at, send, recv):
+        remote(at, at, send, recv, ep=mate).wait_send()
+
+    drain(named.at[pl.ds(0, n_ep - 1)], n_send.at[0], n_recv.at[0])
+    drain(summary.at[pl.ds(0, n_ep - 1)], e_send.at[0], e_recv.at[0])
+    drain(result.at[pl.ds(0, n_ep - 1)], r_send.at[0], r_recv.at[0])
+    drain(tok.at[:, 0], mate_send.at[0], tok_recv.at[0, 0])
+    for d in range(2):
+        @pl.when(ends[d][0])
         def _():
-            along(u).wait_send()
+            drain(tok.at[pl.ds(0, 2), 0], own_send.at[d], tok_recv.at[0, 0])
+
+    @pl.when(jnp.logical_and(ends[0][0], ends[1][0]))
+    def _():
+        drain(tok.at[pl.ds(0, last + 1), 0], on_send.at[0], tok_recv.at[0, 0])
+
+    store_out.wait()
+    store_experts.wait()
 
 
 def shards(
@@ -622,7 +638,7 @@
             jax.ShapeDtypeStruct((count, columns), bf16),
         ),
         in_specs=[vmem] * 4 + [anywhere] * len(operands),
-        out_specs=(vmem, vmem),
+        out_specs=(anywhere, anywhere),
         scratch_shapes=[pltpu.VMEM(a.shape, a.dtype) for a in operands] + [
             pltpu.VMEM((4, merged), f32),
             pltpu.VMEM((rows, merged), f32),
@@ -633,7 +649,7 @@
             pltpu.VMEM((n_tp, 2, rows // 2, channels), bf16),
             pltpu.VMEM((n_ep, 2, count // 2, features), bf16),
             pltpu.VMEM((n_ep, 2, count), jnp.int32),
-            pltpu.VMEM((cap, features), bf16),
+            pltpu.VMEM((2 * cap, features), bf16),
             pltpu.VMEM((n_ep, n_tp, 2, cap, ff // 2), bf16),
             pltpu.VMEM((n_ep, cap, columns), bf16),
             pltpu.VMEM((n_ep, cap, columns), bf16),
@@ -641,10 +657,11 @@
             pltpu.VMEM((count, columns), f32),
             pltpu.VMEM((n_ep * cap, count), bf16),
             pltpu.VMEM((n_ep * cap, count), bf16),
-            dma((len(operands),)), dma((n_ep, 2)), dma((n_ep, 2)), dma((2, 2)),
-            dma((n_ep,)), dma((n_ep,)), dma((n_ep,)), dma((n_ep,)), dma((n_ep,)),
-            dma((2, n_tp)), dma((n_tp, 2)), dma((n_ep, 2, n_tp)), dma((n_ep, n_tp, 2)),
-            dma((n_ep,)), dma((n_ep,)), dma((2, n_tp)), dma((n_tp, 2)),
+            pltpu.VMEM((rows, mixer_weight.shape[1]), bf16),
+            pltpu.VMEM((count, columns), bf16),
+            dma((len(operands),)), dma((2,)), dma((n_ep, 2)), dma((1,)), dma((2,)), dma((1,)),
+            dma((1,)), dma((2,)), dma((1,)), dma((1,)), dma((1,)), dma((4,)),
+            dma((1,)), dma((n_ep, 4)), dma((1,)), dma((1,)), dma((1,)), dma((4,)),
         ],
         compiler_params=pltpu.CompilerParams(
             collective_id=0, has_side_effects=True, vmem_limit_bytes=56 * 1024 * 1024

time: 76.8 us -> 69.5 us (0.905)
  Pallas kernels: 72.7 us -> 65.4 us
    pallas_call x1, Pallas kernels: 72.7 us -> 65.4 us  [shards(): pl.pallas_call(functools.partial(fused_kernel, n_ep, n_tp, states), out_s...]
where the time goes in v2:
time: 69.5 us; the launch traced here: 69.3 us
  Pallas kernels  65.4 us (94%)
  local copies, waits for them, and re-layouts  3.24 us (5%)
    pallas_call x1, Pallas kernels, shards(): pl.pallas_call(functools.partial(fused_kernel, n_ep, n_tp, states), out_s...  65.4 us
    unnamed x2, local copies, waits for them, and re-layouts  3.24 us

profile of v2, /device:TPU:1, one launch (start us, length us, event | category | flops | bytes accessed | tf_op | source)
XLA Modules:
  0.0 69.3 jit_solution(18231450803031959476)
XLA Ops:
  0.6 65.4 %fused.1 = (bf16[256,512]{1,0:T(8,128)(2,1)}, bf16[128,512]{1,0:T(8,128)(2,1)}) custom-call(s32[2,128]{1,0:T(2,128)} %bitcast.21, f32[2,128]{1,0:T(2,128)} %bitcast.22, f32[1,16]{1,0:T(1,128)} %bitcast.23, f32[1,2048]{1,0:T(1,128)} %bitcast.20, bf16[2,64,2048]{2,1,0:T(8,128)(2,1)} %bitcast.16, bf16[256,256]{1,0:T(8,128)(2,1)} %x_hbm.1, f32[16,256]{1,0:T(8,128)} %bitcast.19, ...), custom_call_target="tpu_custom_call" | custom-call | tf_op jit(solution)/shard_map/fused/pallas_call | solution.py:634
  66.0 1.7 %copy.20 = bf16[256,512]{1,0:T(8,128)(2,1)} copy(bf16[256,512]{1,0:T(8,128)(2,1)} %get-tuple-element.4) | data formatting | bytes 524288
  67.7 1.6 %copy.21 = bf16[128,512]{1,0:T(8,128)(2,1)} copy(bf16[128,512]{1,0:T(8,128)(2,1)} %get-tuple-element.5) | data formatting | bytes 262144

commit v3 on v2

--- a/solution.py
+++ b/solution.py
@@ -186,8 +186,8 @@
         units = []
         for u, (source, onward, arrival) in enumerate(found):
             together = max(v for v in range(len(found)) if found[v][2] == arrival)
-            step = 2 * u if end else max(0, 2 * together - 3)
-            units.append((source, onward, step, int(end and u > 1)))
+            ahead = max((3 * together - 1) // 2, 3 * together - 7) if together > 1 else 0
+            units.append((source, onward, 3 * u if end else ahead))
         plan.append(units)
     return plan
 
@@ -201,8 +201,8 @@
     tokens, x_ref, shift_ref, map_ref, readout_ref, weight_ref,
     sgate, sup, sdown, gate, up, down,
     table, mag, push_re, push_im, pre, summary, active,
-    tok, named, picked, hidden, result, returned, shared, common, high, low, out_v, experts_v,
-    load, store, tok_recv, mate_send, own_send, on_send, n_send, n_recv,
+    tok, named, ranks, picked, hidden, result, returned, shared, common, high, low,
+    load, tok_recv, mate_send, own_send, on_send, n_send, n_recv,
     e_send, e_recv, a_send, a_recv, h_send, h_recv, r_send, r_recv, s_send, s_recv,
 ):
     ep = lax.axis_index("ep")
@@ -236,8 +236,6 @@
     loads = [pltpu.make_async_copy(a, b, load.at[i]) for i, (a, b) in enumerate(pairs)]
     for copy in loads:
         copy.start()
-    store_out = pltpu.make_async_copy(out_v, out_ref, store.at[0])
-    store_experts = pltpu.make_async_copy(experts_v, experts_ref, store.at[1])
     def across(dy, dx):
         return lax.rem(y + dy, side) * side + lax.rem(x + dx, side)
 
@@ -313,7 +311,7 @@
     def own(j, d):
         return piece(2 * chip + j, core, own_send.at[d], ends[d][1])
 
-    for j in range(2):
+    def depart(j):
         @pl.when(core != j)
         def _():
             piece(2 * chip + j, core, mate_send.at[0], mate).wait_recv()
@@ -322,6 +320,8 @@
             @pl.when(ends[d][0])
             def _():
                 own(j, d).start()
+
+    depart(0)
 
     def shared_hidden():
         for copy in loads[1:3]:
@@ -338,20 +338,16 @@
     slots = iota((cap, count), 0).astype(jnp.float32)
 
     def member(names, expert):
-        return jnp.logical_or(names[0:1] == expert, names[1:2] == expert)
+        return jnp.where(jnp.logical_or(names[0:1] == expert, names[1:2] == expert), 1.0, 0.0)
 
     def seats(mine):
-        ones = jnp.where(mine, 1.0, 0.0)
-        ranks = dot(ones.astype(jnp.bfloat16), later)
-        return jnp.where(mine, ranks - 1.0, -1.0)
-
-    tile = min(half, 256)
+        return jnp.where(mine > 0.0, dot(mine.astype(jnp.bfloat16), later) - 1.0, -1.0)
+
+    tile = half
 
     def process(*group):
         for i, s in enumerate(group):
-            names = named[s]
-            place = seats(jnp.broadcast_to(member(names, ep), (SUBLANES, count)))
-            chosen = (slots == place[0:1]).astype(jnp.bfloat16)
+            chosen = (slots == ranks[s]).astype(jnp.bfloat16)
             picked[i * cap : (i + 1) * cap, :] = dot(
                 chosen, tok[s].reshape(count, features)
             ).astype(jnp.bfloat16)
@@ -372,7 +368,7 @@
     def back(s):
         return remote(result.at[s], returned.at[ep], r_send.at[0], r_recv.at[0], ep=s)
 
-    def project(*group, before=None):
+    def project(*group):
         def part(q):
             total = None
             for h in range(2):
@@ -382,8 +378,6 @@
             return total
 
         total = part(tp)
-        if before is not None:
-            before()
         for s in group:
             hidden_of(s).near()
         for o in range(1, side):
@@ -417,15 +411,24 @@
                 summary.at[ep], summary.at[ep], e_send.at[0], e_recv.at[0], ep=target
             ).start()
 
+    def rank(first, number):
+        mine = [member(named[first + i], ep) for i in range(number)]
+        mine += [mine[0]] * (-number % SUBLANES)
+        place = seats(jnp.concatenate(mine, axis=0))
+        for i in range(number):
+            ranks[first + i] = place[i : i + 1]
+
     def gain_blocks():
         names = routes_ref[...]
         level = gains_ref[...]
+        wanted = [member(names, e) for e in range(n_ep)]
+        wanted += [wanted[0]] * (-n_ep % SUBLANES)
+        places = seats(jnp.concatenate(wanted, axis=0))
         for e in range(n_ep):
-            place = seats(jnp.broadcast_to(member(names, e), (SUBLANES, count)))
             weight = jnp.where(names[0:1] == e, level[0:1], 0.0) + jnp.where(
                 names[1:2] == e, level[1:2], 0.0
             )
-            wide = jnp.where(slots == place[0:1], weight, 0.0)
+            wide = jnp.where(slots == places[e : e + 1], weight, 0.0)
             top, rest = halves(wide)
             high[e * cap : (e + 1) * cap, :] = top
             low[e * cap : (e + 1) * cap, :] = rest
@@ -457,8 +460,7 @@
             a = active[q].reshape(rows, channels)
             part = dot(a, weight_ref[q * channels : (q + 1) * channels, :])
             total = part if total is None else total + part
-        out_v[...] = total.astype(out_v.dtype)
-        store_out.start()
+        out_ref[...] = total.astype(out_ref.dtype)
         shared_out.near()
         shared_out.far()
         loads[11].wait()
@@ -482,7 +484,6 @@
     source = [here(u, 0) for u in range(last + 1)]
     onward = [here(u, 1) for u in range(last + 1)]
     steps = [here(u, 2) for u in range(last + 1)]
-    early = [here(u, 3) for u in range(last + 1)]
 
     def along(u):
         target = 2 * jnp.maximum(onward[u], 0) + core
@@ -510,16 +511,19 @@
             hidden_of(s).forward()
 
     shared_hidden()
+    depart(1)
     for copy in loads[3:5]:
         copy.wait()
     ready(mate)
     remote(routes_ref, named.at[mate], n_send.at[0], n_recv.at[0], ep=mate).wait_recv()
+    rank(2 * chip, 2)
     process(*groups[0])
     scan_block()
     gain_blocks()
     shared_out.forward()
     rest = named.at[pl.ds(0, n_ep - 2)]
     remote(rest, rest, n_send.at[0], n_recv.at[1], ep=mate).wait_recv()
+    rank(0, n_ep)
 
     def arrivals(step):
         for v in range(last + 1):
@@ -529,38 +533,33 @@
                     pass_on(v)
 
     for u in range(last + 1):
-        arrivals(2 * u)
-
-        @pl.when(early[u] == 1)
-        def _():
+        arrivals(3 * u)
+        if u == last:
             forward(groups[u])
-
         ready(source[u])
         process(source[u])
-        arrivals(2 * u + 1)
-
-        @pl.when(early[u] == 0)
-        def _():
+        arrivals(3 * u + 1)
+        if u == min(1, last):
+            scan_states()
+        if u < last:
             forward(groups[u])
-
+        if u == min(2, last):
+            active_out.forward()
         if u == 1:
             loads[8].wait()
         if u > 0:
             project(*groups[u - 1])
-        if u == min(2, last):
-            scan_states()
-        if u == min(3, last):
-            active_out.forward()
+        arrivals(3 * u + 2)
         if u == min(4, last):
             mix()
+    forward(groups[last + 1])
     project(*groups[last])
-    project(*groups[last + 1], before=functools.partial(forward, groups[last + 1]))
+    project(*groups[last + 1])
     rest = returned.at[pl.ds(0, n_ep - 1)]
     remote(rest, rest, r_send.at[0], r_recv.at[0], ep=mate).wait_recv()
     back_rows = returned[...].reshape(n_ep * cap, returned.shape[2])
     routed = dot(high[...], back_rows, TN) + dot(low[...], back_rows, TN)
-    experts_v[...] = (common[...] + routed).astype(experts_v.dtype)
-    store_experts.start()
+    experts_ref[...] = (common[...] + routed).astype(experts_ref.dtype)
     shared_out.drain(shared.at[pl.ds(0, n_tp - 1)])
     active_out.drain(active.at[pl.ds(0, n_tp - 1)])
     hidden_of(ep).drain(hidden.at[:, pl.ds(0, n_tp - 1)])
@@ -580,9 +579,6 @@
     @pl.when(jnp.logical_and(ends[0][0], ends[1][0]))
     def _():
         drain(tok.at[pl.ds(0, last + 1), 0], on_send.at[0], tok_recv.at[0, 0])
-
-    store_out.wait()
-    store_experts.wait()
 
 
 def shards(
@@ -634,11 +630,11 @@
     return tuple(pl.pallas_call(
         functools.partial(fused_kernel, n_ep, n_tp, states),
         out_shape=(
-            jax.ShapeDtypeStruct((rows, mixer_weight.shape[1]), bf16),
-            jax.ShapeDtypeStruct((count, columns), bf16),
+            pltpu.VMEM((rows, mixer_weight.shape[1]), bf16),
+            pltpu.VMEM((count, columns), bf16),
         ),
         in_specs=[vmem] * 4 + [anywhere] * len(operands),
-        out_specs=(anywhere, anywhere),
+        out_specs=(vmem, vmem),
         scratch_shapes=[pltpu.VMEM(a.shape, a.dtype) for a in operands] + [
             pltpu.VMEM((4, merged), f32),
             pltpu.VMEM((rows, merged), f32),
@@ -649,6 +645,7 @@
             pltpu.VMEM((n_tp, 2, rows // 2, channels), bf16),
             pltpu.VMEM((n_ep, 2, count // 2, features), bf16),
             pltpu.VMEM((n_ep, 2, count), jnp.int32),
+            pltpu.VMEM((n_ep, 1, count), f32),
             pltpu.VMEM((2 * cap, features), bf16),
             pltpu.VMEM((n_ep, n_tp, 2, cap, ff // 2), bf16),
             pltpu.VMEM((n_ep, cap, columns), bf16),
@@ -657,9 +654,7 @@
             pltpu.VMEM((count, columns), f32),
             pltpu.VMEM((n_ep * cap, count), bf16),
             pltpu.VMEM((n_ep * cap, count), bf16),
-            pltpu.VMEM((rows, mixer_weight.shape[1]), bf16),
-            pltpu.VMEM((count, columns), bf16),
-            dma((len(operands),)), dma((2,)), dma((n_ep, 2)), dma((1,)), dma((2,)), dma((1,)),
+            dma((len(operands),)), dma((n_ep, 2)), dma((1,)), dma((2,)), dma((1,)),
             dma((1,)), dma((2,)), dma((1,)), dma((1,)), dma((1,)), dma((4,)),
             dma((1,)), dma((n_ep, 4)), dma((1,)), dma((1,)), dma((1,)), dma((4,)),
         ],

time: 69.5 us -> 62.1 us (0.89)
  Pallas kernels: 65.4 us -> 59.7 us
  local copies, waits for them, and re-layouts: 3.24 us -> 1.36 us
    pallas_call x1, Pallas kernels: 65.4 us -> 59.7 us  [shards(): pl.pallas_call(functools.partial(fused_kernel, n_ep, n_tp, states), out_s...]
    unnamed x2, local copies, waits for them, and re-layouts: 3.24 us -> 1.36 us
where the time goes in v3:
time: 62.1 us; the launch traced here: 61.7 us
  Pallas kernels  59.7 us (96%)
  local copies, waits for them, and re-layouts  1.36 us (2%)
  between operations  0.65 us (1%)
    pallas_call x1, Pallas kernels, shards(): pl.pallas_call(functools.partial(fused_kernel, n_ep, n_tp, states), out_s...  59.7 us
    unnamed x2, local copies, waits for them, and re-layouts  1.36 us

profile of v3, /device:TPU:1, one launch (start us, length us, event | category | flops | bytes accessed | tf_op | source)
XLA Modules:
  0.0 61.7 jit_solution(3560554670294309939)
XLA Ops:
  0.6 59.7 %fused.1 = (bf16[256,512]{1,0:T(8,128)(2,1)S(1)}, bf16[128,512]{1,0:T(8,128)(2,1)S(1)}) custom-call(s32[2,128]{1,0:T(2,128)} %bitcast.21, f32[2,128]{1,0:T(2,128)} %bitcast.22, f32[1,16]{1,0:T(1,128)} %bitcast.23, f32[1,2048]{1,0:T(1,128)} %bitcast.20, bf16[2,64,2048]{2,1,0:T(8,128)(2,1)} %bitcast.16, bf16[256,256]{1,0:T(8,128)(2,1)} %x_hbm.1, ...), custom_call_target="tpu_custom_call" | custom-call | tf_op jit(solution)/shard_map/fused/pallas_call | solution.py:630
  60.3 0.7 %copy.20 = bf16[256,512]{1,0:T(8,128)(2,1)} copy(bf16[256,512]{1,0:T(8,128)(2,1)S(1)} %get-tuple-element.2) | data formatting | bytes 524288
  61.0 0.7 %copy.21 = bf16[128,512]{1,0:T(8,128)(2,1)} copy(bf16[128,512]{1,0:T(8,128)(2,1)S(1)} %get-tuple-element.3) | data formatting | bytes 262144

commit v4 on v3

--- a/solution.py
+++ b/solution.py
@@ -118,17 +118,22 @@
     return lax.fori_loop(0, rows // SUBLANES, one, (start_re, start_im, product))
 
 
+def power(wr, wi, steps):
+    reached = 1
+    while reached < steps:
+        wr, wi = times(wr, wi, wr, wi)
+        reached *= 2
+    return wr, wi
+
+
 def join(table_ref, ends_re, ends_im, product, pre, steps):
     merged = ends_re.shape[1]
-    wr, wi = table_ref[0:1, :], table_ref[1:2, :]
-    power = 1
-    while power < steps:
-        wr, wi = times(wr, wi, wr, wi)
-        power *= 2
+    wr, wi = power(table_ref[0:1, :], table_ref[1:2, :], steps)
     cr = jnp.zeros((1, merged), jnp.float32)
     ci = cr
     ar = cr + 1.0
     ai = cr
+    whole = cr + 1.0
     for s in range(SUBLANES):
         for i, v in enumerate((cr, ci, ar, ai)):
             pre[i, s : s + 1, :] = v
@@ -137,7 +142,13 @@
         tr, ti = times(fr, fi, cr, ci)
         cr, ci = tr + ends_re[s : s + 1], ti + ends_im[s : s + 1]
         ar, ai = times(fr, fi, ar, ai)
-    return cr, ci, ar, ai
+        whole = whole * level
+    return cr, ci, whole
+
+
+def follow(part, turn, re, im):
+    re, im = times(turn[0], turn[1], re, im)
+    return part[2:3] * re + part[0:1], part[2:3] * im + part[1:2]
 
 
 def read_states(readout_ref, push_re, push_im, states):
@@ -200,10 +211,10 @@
     out_ref, experts_ref,
     tokens, x_ref, shift_ref, map_ref, readout_ref, weight_ref,
     sgate, sup, sdown, gate, up, down,
-    table, mag, push_re, push_im, pre, summary, active,
+    table, mag, push_re, push_im, pre, blocks, summary, active,
     tok, named, ranks, picked, hidden, result, returned, shared, common, high, low,
     load, tok_recv, mate_send, own_send, on_send, n_send, n_recv,
-    e_send, e_recv, a_send, a_recv, h_send, h_recv, r_send, r_recv, s_send, s_recv,
+    b_send, b_recv, e_send, e_recv, a_send, a_recv, h_send, h_recv, r_send, r_recv, s_send, s_recv,
 ):
     ep = lax.axis_index("ep")
     tp = lax.axis_index("tp")
@@ -217,8 +228,11 @@
     mate = ep + 1 - 2 * core
     side = math.isqrt(n_tp)
     y, x = tp // side, lax.rem(tp, side)
-    half = hidden.shape[4]
-
+    pieces, quarter = hidden.shape[2], hidden.shape[4]
+    half = 2 * quarter
+
+    first_load = pltpu.make_async_copy(input_hbm, tokens, load.at[0])
+    first_load.start()
     barrier = pltpu.get_barrier_semaphore()
     for d in range(1, n_ep):
         pl.semaphore_signal(
@@ -234,7 +248,7 @@
         (readout_hbm, readout_ref), (weight_hbm, weight_ref), (sdown_hbm, sdown),
     )
     loads = [pltpu.make_async_copy(a, b, load.at[i]) for i, (a, b) in enumerate(pairs)]
-    for copy in loads:
+    for copy in loads[1:]:
         copy.start()
     def across(dy, dx):
         return lax.rem(y + dy, side) * side + lax.rem(x + dx, side)
@@ -244,32 +258,37 @@
     class Share:
         def __init__(self, buffer, send, recv):
             self.buffer, self.send, self.recv = buffer, send, recv
+            self.pieces = buffer.shape[1]
 
         def copy(self, source, h, to, k):
             at = self.buffer.at[source, h]
             return remote(at, at, self.send, self.recv.at[k], tp=to)
 
         def start(self, h):
-            for o in range(1, side):
-                self.copy(tp, h, peers[0, o], 0 if h == 0 else 2).start()
-                self.copy(tp, h, peers[o, 0], 1 if h == 1 else 2).start()
+            for first in (True, False):
+                for o in range(1, side):
+                    row, column = (h, h + 1) if first else (h + 1, h)
+                    k = h // 2 if first else self.pieces // 2
+                    self.copy(tp, row, peers[0, o], k).start()
+                    self.copy(tp, column, peers[o, 0], k).start()
 
         def wait(self, at, k):
             remote(at, at, self.send, self.recv.at[k], tp=peers[0, 1]).wait_recv()
 
         def forward(self):
-            for h in range(2):
-                self.wait(self.buffer.at[pl.ds(0, side - 1), h], h)
+            far = self.pieces // 2 + 1
+            for h in range(0, self.pieces, 2):
+                self.wait(self.buffer.at[pl.ds(0, side - 1), pl.ds(h, 2)], h // 2)
                 for o in range(1, side):
                     for d in range(1, side):
-                        source, to = ((0, o), (d, 0)) if h == 0 else ((o, 0), (0, d))
-                        self.copy(peers[source], h, peers[to], 3).start()
+                        self.copy(peers[0, o], h, peers[d, 0], far).start()
+                        self.copy(peers[o, 0], h + 1, peers[0, d], far).start()
 
         def near(self):
-            self.wait(self.buffer.at[pl.ds(0, side - 1)], 2)
+            self.wait(self.buffer.at[pl.ds(0, side - 1)], self.pieces // 2)
 
         def far(self):
-            self.wait(self.buffer.at[pl.ds(0, (side - 1) ** 2)], 3)
+            self.wait(self.buffer.at[pl.ds(0, (side - 1) ** 2)], self.pieces // 2 + 1)
 
         def drain(self, at):
             remote(at, at, self.send, self.recv.at[0], tp=peers[0, 1]).wait_send()
@@ -280,7 +299,7 @@
     shared_out = Share(shared, s_send.at[0], s_recv)
     active_out = Share(active, a_send.at[0], a_recv)
 
-    loads[0].wait()
+    first_load.wait()
     block = 16
     scale = gain_ref[...]
 
@@ -331,8 +350,7 @@
         shared[tp] = (v / (1.0 + jnp.exp(-v)) * dot(a, sup[...])).astype(jnp.bfloat16).reshape(
             shared.shape[1:]
         )
-        for h in range(2):
-            shared_out.start(h)
+        shared_out.start(0)
 
     later = (iota((count, count), 0) <= iota((count, count), 1)).astype(jnp.bfloat16)
     slots = iota((cap, count), 0).astype(jnp.float32)
@@ -342,8 +360,6 @@
 
     def seats(mine):
         return jnp.where(mine > 0.0, dot(mine.astype(jnp.bfloat16), later) - 1.0, -1.0)
-
-    tile = half
 
     def process(*group):
         for i, s in enumerate(group):
@@ -351,27 +367,25 @@
             picked[i * cap : (i + 1) * cap, :] = dot(
                 chosen, tok[s].reshape(count, features)
             ).astype(jnp.bfloat16)
-        for h in range(2):
-            @pl.loop(0, half // tile)
-            def _(n):
-                inner = pl.ds(pl.multiple_of(n * tile, tile), tile)
-                at = pl.ds(pl.multiple_of(h * half + n * tile, tile), tile)
-                a = picked[: len(group) * cap, :]
-                v = dot(a, gate[:, at])
-                v = (v / (1.0 + jnp.exp(-v)) * dot(a, up[:, at])).astype(jnp.bfloat16)
-                for i, s in enumerate(group):
-                    hidden[s, tp, h, :, inner] = v[i * cap : (i + 1) * cap]
-
-            for s in group:
+        a = picked[: len(group) * cap, :]
+        for h in range(0, pieces, 2):
+            at = slice(h * quarter, h * quarter + half)
+            v = dot(a, gate[:, at])
+            v = (v / (1.0 + jnp.exp(-v)) * dot(a, up[:, at])).astype(jnp.bfloat16)
+            for i, s in enumerate(group):
+                for k in range(2):
+                    hidden[s, tp, h + k] = v[
+                        i * cap : (i + 1) * cap, k * quarter : (k + 1) * quarter
+                    ]
                 hidden_of(s).start(h)
 
     def back(s):
         return remote(result.at[s], returned.at[ep], r_send.at[0], r_recv.at[0], ep=s)
 
-    def project(*group):
+    def project(*group, now=True):
         def part(q):
             total = None
-            for h in range(2):
+            for h in range(pieces):
                 a = jnp.concatenate([hidden[s, q, h] for s in group], axis=0)
                 one = dot(a, down[q, h])
                 total = one if total is None else total + one
@@ -393,7 +407,7 @@
         if len(group) == 2:
             returned[ep] = result[ep]
             back(mate).start()
-        else:
+        elif now:
             back(group[0]).start()
 
     def scan_block():
@@ -405,11 +419,38 @@
         ends_re, ends_im, product = sweep(table, mag, push_re, push_im, zero, zero, False)
         end = join(table, ends_re, ends_im, product, pre, rows // SUBLANES)
         for i, v in enumerate(end):
-            summary[ep, i : i + 1, :] = v
-        for target in strangers + [mate]:
-            remote(
-                summary.at[ep], summary.at[ep], e_send.at[0], e_recv.at[0], ep=target
-            ).start()
+            blocks[core, i : i + 1, :] = v
+
+        @pl.when(core == 0)
+        def _():
+            first_block().start()
+
+    def first_block():
+        return remote(blocks.at[0], blocks.at[0], b_send.at[0], b_recv.at[0], ep=mate)
+
+    def whole_chip(d, c):
+        return remote(
+            summary.at[chip], summary.at[chip], e_send.at[d], e_recv.at[chip],
+            ep=lax.rem(2 * (chip + d) + c, n_ep),
+        )
+
+    def turn_over(count):
+        return power(table[0:1, :], table[1:2, :], count)
+
+    def scan_chip():
+        @pl.when(core == 1)
+        def _():
+            first_block().wait_recv()
+            first = blocks[0]
+            part = blocks[1]
+            re, im = follow(part, turn_over(rows), first[0:1], first[1:2])
+            for i, v in enumerate((re, im, first[2:3] * part[2:3])):
+                summary[chip, i : i + 1, :] = v
+            for d in range(1, chips):
+                @pl.when(chip + d < chips)
+                def _():
+                    for c in range(2):
+                        whole_chip(d, c).start()
 
     def rank(first, number):
         mine = [member(named[first + i], ep) for i in range(number)]
@@ -434,22 +475,28 @@
             low[e * cap : (e + 1) * cap, :] = rest
 
     def scan_states():
-        rest = summary.at[pl.ds(0, n_ep - 1)]
-        remote(rest, rest, e_send.at[0], e_recv.at[0], ep=mate).wait_recv()
-
-        def fold(e, carry):
-            part = summary[e]
-            re, im = times(part[2:3], part[3:4], carry[0], carry[1])
-            return re + part[0:1], im + part[1:2]
+        for k in range(chips - 1):
+            @pl.when(k < chip)
+            def _():
+                remote(
+                    summary.at[k], summary.at[k], e_send.at[0], e_recv.at[k], ep=mate
+                ).wait_recv()
+
+        turn = turn_over(2 * rows)
+
+        def fold(k, carry):
+            return follow(summary[k], turn, *carry)
 
         nothing = jnp.zeros((1, merged), jnp.float32)
-        in_re, in_im = lax.fori_loop(0, ep, fold, (nothing, nothing))
+        in_re, in_im = lax.fori_loop(0, chip, fold, (nothing, nothing))
+        step_re, step_im = follow(blocks[0], turn_over(rows), in_re, in_im)
+        in_re = jnp.where(core == 1, step_re, in_re)
+        in_im = jnp.where(core == 1, step_im, in_im)
         add_re, add_im = times(pre[2], pre[3], in_re, in_im)
         sweep(table, mag, push_re, push_im, pre[0] + add_re, pre[1] + add_im, True)
         loads[9].wait()
         active[tp] = read_states(readout_ref, push_re, push_im, states).reshape(active.shape[1:])
-        for h in range(2):
-            active_out.start(h)
+        active_out.start(0)
 
     def mix():
         active_out.near()
@@ -520,6 +567,7 @@
     process(*groups[0])
     scan_block()
     gain_blocks()
+    scan_chip()
     shared_out.forward()
     rest = named.at[pl.ds(0, n_ep - 2)]
     remote(rest, rest, n_send.at[0], n_recv.at[1], ep=mate).wait_recv()
@@ -548,12 +596,14 @@
         if u == 1:
             loads[8].wait()
         if u > 0:
-            project(*groups[u - 1])
+            project(*groups[u - 1], now=u != 2)
         arrivals(3 * u + 2)
+        if u == 2:
+            back(source[0]).start()
         if u == min(4, last):
             mix()
+    project(*groups[last])
     forward(groups[last + 1])
-    project(*groups[last])
     project(*groups[last + 1])
     rest = returned.at[pl.ds(0, n_ep - 1)]
     remote(rest, rest, r_send.at[0], r_recv.at[0], ep=mate).wait_recv()
@@ -568,7 +618,16 @@
         remote(at, at, send, recv, ep=mate).wait_send()
 
     drain(named.at[pl.ds(0, n_ep - 1)], n_send.at[0], n_recv.at[0])
-    drain(summary.at[pl.ds(0, n_ep - 1)], e_send.at[0], e_recv.at[0])
+
+    @pl.when(core == 0)
+    def _():
+        first_block().wait_send()
+
+    for d in range(1, chips):
+        @pl.when(jnp.logical_and(core == 1, chip + d < chips))
+        def _():
+            drain(summary.at[pl.ds(0, 2)], e_send.at[d], e_recv.at[0])
+
     drain(result.at[pl.ds(0, n_ep - 1)], r_send.at[0], r_recv.at[0])
     drain(tok.at[:, 0], mate_send.at[0], tok_recv.at[0, 0])
     for d in range(2):
@@ -625,7 +684,7 @@
         shared_down,
         expert_switch_matrix.reshape(features, ff),
         up_weight.reshape(features, ff),
-        down_weight.reshape(n_tp, 2, ff // 2, columns),
+        down_weight.reshape(n_tp, 4, ff // 4, columns),
     )
     return tuple(pl.pallas_call(
         functools.partial(fused_kernel, n_ep, n_tp, states),
@@ -641,13 +700,14 @@
             pltpu.VMEM((rows, merged), f32),
             pltpu.VMEM((rows, merged), f32),
             pltpu.VMEM((4, SUBLANES, merged), f32),
-            pltpu.VMEM((n_ep, 4, merged), f32),
+            pltpu.VMEM((2, 3, merged), f32),
+            pltpu.VMEM((n_ep // 2, 3, merged), f32),
             pltpu.VMEM((n_tp, 2, rows // 2, channels), bf16),
             pltpu.VMEM((n_ep, 2, count // 2, features), bf16),
             pltpu.VMEM((n_ep, 2, count), jnp.int32),
             pltpu.VMEM((n_ep, 1, count), f32),
             pltpu.VMEM((2 * cap, features), bf16),
-            pltpu.VMEM((n_ep, n_tp, 2, cap, ff // 2), bf16),
+            pltpu.VMEM((n_ep, n_tp, 4, cap, ff // 4), bf16),
             pltpu.VMEM((n_ep, cap, columns), bf16),
             pltpu.VMEM((n_ep, cap, columns), bf16),
             pltpu.VMEM((n_tp, 2, count // 2, shared_ff), bf16),
@@ -655,8 +715,9 @@
             pltpu.VMEM((n_ep * cap, count), bf16),
             pltpu.VMEM((n_ep * cap, count), bf16),
             dma((len(operands),)), dma((n_ep, 2)), dma((1,)), dma((2,)), dma((1,)),
-            dma((1,)), dma((2,)), dma((1,)), dma((1,)), dma((1,)), dma((4,)),
-            dma((1,)), dma((n_ep, 4)), dma((1,)), dma((1,)), dma((1,)), dma((4,)),
+            dma((1,)), dma((2,)), dma((1,)), dma((1,)), dma((n_ep // 2,)), dma((n_ep // 2,)),
+            dma((1,)), dma((3,)),
+            dma((1,)), dma((n_ep, 4)), dma((1,)), dma((1,)), dma((1,)), dma((3,)),
         ],
         compiler_params=pltpu.CompilerParams(
             collective_id=0, has_side_effects=True, vmem_limit_bytes=56 * 1024 * 1024

time: 62.1 us -> 60.6 us (0.976)
  Pallas kernels: 59.7 us -> 58.4 us
    pallas_call x1, Pallas kernels: 59.7 us -> 58.4 us  [shards(): pl.pallas_call(functools.partial(fused_kernel, n_ep, n_tp, states), out_s...]
where the time goes in v4:
time: 60.6 us; the launch traced here: 60.4 us
  Pallas kernels  58.4 us (96%)
  local copies, waits for them, and re-layouts  1.36 us (2%)
  between operations  0.65 us (1%)
    pallas_call x1, Pallas kernels, shards(): pl.pallas_call(functools.partial(fused_kernel, n_ep, n_tp, states), out_s...  58.4 us
    unnamed x2, local copies, waits for them, and re-layouts  1.36 us

profile of v4, /device:TPU:1, one launch (start us, length us, event | category | flops | bytes accessed | tf_op | source)
XLA Modules:
  0.0 60.4 jit_solution(15166503920900666309)
XLA Ops:
  0.6 58.4 %fused.1 = (bf16[256,512]{1,0:T(8,128)(2,1)S(1)}, bf16[128,512]{1,0:T(8,128)(2,1)S(1)}) custom-call(s32[2,128]{1,0:T(2,128)} %bitcast.21, f32[2,128]{1,0:T(2,128)} %bitcast.22, f32[1,16]{1,0:T(1,128)} %bitcast.23, f32[1,2048]{1,0:T(1,128)} %bitcast.20, bf16[2,64,2048]{2,1,0:T(8,128)(2,1)} %bitcast.16, bf16[256,256]{1,0:T(8,128)(2,1)} %x_hbm.1, ...), custom_call_target="tpu_custom_call" | custom-call | tf_op jit(solution)/shard_map/fused/pallas_call | solution.py:689
  59.0 0.7 %copy.20 = bf16[256,512]{1,0:T(8,128)(2,1)} copy(bf16[256,512]{1,0:T(8,128)(2,1)S(1)} %get-tuple-element.2) | data formatting | bytes 524288
  59.7 0.7 %copy.21 = bf16[128,512]{1,0:T(8,128)(2,1)} copy(bf16[128,512]{1,0:T(8,128)(2,1)S(1)} %get-tuple-element.3) | data formatting | bytes 262144

commit v5 on v4

--- a/solution.py
+++ b/solution.py
@@ -205,11 +205,10 @@
 
 def fused_kernel(
     n_ep, n_tp, states,
-    routes_ref, gains_ref, rate_ref, gain_ref,
-    input_hbm, x_hbm, shift_hbm, map_hbm, readout_hbm, weight_hbm,
+    routes_hbm, gains_hbm, rate_hbm, gain_hbm, input_hbm, x_hbm, shift_hbm, map_hbm, readout_hbm, weight_hbm,
     sgate_hbm, sup_hbm, sdown_hbm, gate_hbm, up_hbm, down_hbm,
     out_ref, experts_ref,
-    tokens, x_ref, shift_ref, map_ref, readout_ref, weight_ref,
+    routes_ref, gains_ref, rate_ref, gain_ref, tokens, x_ref, shift_ref, map_ref, readout_ref, weight_ref,
     sgate, sup, sdown, gate, up, down,
     table, mag, push_re, push_im, pre, blocks, summary, active,
     tok, named, ranks, picked, hidden, result, returned, shared, common, high, low,
@@ -231,8 +230,15 @@
     pieces, quarter = hidden.shape[2], hidden.shape[4]
     half = 2 * quarter
 
-    first_load = pltpu.make_async_copy(input_hbm, tokens, load.at[0])
-    first_load.start()
+    first_loads = [
+        pltpu.make_async_copy(a, b, load.at[i])
+        for i, (a, b) in enumerate((
+            (input_hbm, tokens), (gain_hbm, gain_ref), (routes_hbm, routes_ref),
+            (gains_hbm, gains_ref), (rate_hbm, rate_ref),
+        ))
+    ]
+    for copy in first_loads:
+        copy.start()
     barrier = pltpu.get_barrier_semaphore()
     for d in range(1, n_ep):
         pl.semaphore_signal(
@@ -243,12 +249,15 @@
             barrier, inc=1, device_id={"tp": lax.rem(tp + d, n_tp)}, device_id_type=MESH
         )
     pairs = (
-        (input_hbm, tokens), (sgate_hbm, sgate), (sup_hbm, sup), (gate_hbm, gate), (up_hbm, up),
+        (sgate_hbm, sgate), (sup_hbm, sup), (gate_hbm, gate), (up_hbm, up),
         (x_hbm, x_ref), (shift_hbm, shift_ref), (map_hbm, map_ref), (down_hbm, down),
         (readout_hbm, readout_ref), (weight_hbm, weight_ref), (sdown_hbm, sdown),
     )
-    loads = [pltpu.make_async_copy(a, b, load.at[i]) for i, (a, b) in enumerate(pairs)]
-    for copy in loads[1:]:
+    loads = [
+        pltpu.make_async_copy(a, b, load.at[len(first_loads) + i])
+        for i, (a, b) in enumerate(pairs)
+    ]
+    for copy in loads:
         copy.start()
     def across(dy, dx):
         return lax.rem(y + dy, side) * side + lax.rem(x + dx, side)
@@ -265,12 +274,14 @@
             return remote(at, at, self.send, self.recv.at[k], tp=to)
 
         def start(self, h):
-            for first in (True, False):
-                for o in range(1, side):
-                    row, column = (h, h + 1) if first else (h + 1, h)
-                    k = h // 2 if first else self.pieces // 2
-                    self.copy(tp, row, peers[0, o], k).start()
-                    self.copy(tp, column, peers[o, 0], k).start()
+            for o in range(1, side):
+                self.copy(tp, h, peers[0, o], h // 2).start()
+                self.copy(tp, h + 1, peers[o, 0], h // 2).start()
+            if h + 2 == self.pieces:
+                for g in range(0, self.pieces, 2):
+                    for o in range(1, side):
+                        self.copy(tp, g + 1, peers[0, o], self.pieces // 2).start()
+                        self.copy(tp, g, peers[o, 0], self.pieces // 2).start()
 
         def wait(self, at, k):
             remote(at, at, self.send, self.recv.at[k], tp=peers[0, 1]).wait_recv()
@@ -299,7 +310,8 @@
     shared_out = Share(shared, s_send.at[0], s_recv)
     active_out = Share(active, a_send.at[0], a_recv)
 
-    first_load.wait()
+    for copy in first_loads:
+        copy.wait()
     block = 16
     scale = gain_ref[...]
 
@@ -343,7 +355,7 @@
     depart(0)
 
     def shared_hidden():
-        for copy in loads[1:3]:
+        for copy in loads[0:2]:
             copy.wait()
         a = tok[ep].reshape(count, features)
         v = dot(a, sgate[...])
@@ -411,7 +423,7 @@
             back(group[0]).start()
 
     def scan_block():
-        for copy in loads[5:8]:
+        for copy in loads[4:7]:
             copy.wait()
         column = fill_table(rate_ref, table, states)
         drive_into(x_ref, column, shift_ref, map_ref, table, mag, push_re, push_im, states)
@@ -494,14 +506,14 @@
         in_im = jnp.where(core == 1, step_im, in_im)
         add_re, add_im = times(pre[2], pre[3], in_re, in_im)
         sweep(table, mag, push_re, push_im, pre[0] + add_re, pre[1] + add_im, True)
-        loads[9].wait()
+        loads[8].wait()
         active[tp] = read_states(readout_ref, push_re, push_im, states).reshape(active.shape[1:])
         active_out.start(0)
 
     def mix():
         active_out.near()
         active_out.far()
-        loads[10].wait()
+        loads[9].wait()
         total = None
         for q in range(n_tp):
             a = active[q].reshape(rows, channels)
@@ -510,7 +522,7 @@
         out_ref[...] = total.astype(out_ref.dtype)
         shared_out.near()
         shared_out.far()
-        loads[11].wait()
+        loads[10].wait()
         width = shared.shape[3]
         total = None
         for q in range(n_tp):
@@ -559,7 +571,7 @@
 
     shared_hidden()
     depart(1)
-    for copy in loads[3:5]:
+    for copy in loads[2:4]:
         copy.wait()
     ready(mate)
     remote(routes_ref, named.at[mate], n_send.at[0], n_recv.at[0], ep=mate).wait_recv()
@@ -580,21 +592,31 @@
                 def _():
                     pass_on(v)
 
+    end = jnp.logical_or(chip == 0, chip == chips - 1)
     for u in range(last + 1):
         arrivals(3 * u)
-        if u == last:
+        if 1 < u == last:
             forward(groups[u])
         ready(source[u])
         process(source[u])
         arrivals(3 * u + 1)
         if u == min(1, last):
+            @pl.when(end)
+            def _():
+                forward(groups[u])
+
             scan_states()
-        if u < last:
+
+            @pl.when(jnp.logical_not(end))
+            def _():
+                forward(groups[u])
+
+        elif u < last:
             forward(groups[u])
         if u == min(2, last):
             active_out.forward()
         if u == 1:
-            loads[8].wait()
+            loads[7].wait()
         if u > 0:
             project(*groups[u - 1], now=u != 2)
         arrivals(3 * u + 2)
@@ -673,6 +695,10 @@
     anywhere = pl.BlockSpec(memory_space=pl.ANY)
     dma = pltpu.SemaphoreType.DMA
     operands = (
+        routes.T,
+        route_weight.T,
+        log_step.reshape(1, groups),
+        norm_gain.reshape(1, features),
         expert_input.reshape(2, count // 2, features),
         mixer_input,
         decay_shift.T,
@@ -692,7 +718,7 @@
             pltpu.VMEM((rows, mixer_weight.shape[1]), bf16),
             pltpu.VMEM((count, columns), bf16),
         ),
-        in_specs=[vmem] * 4 + [anywhere] * len(operands),
+        in_specs=[anywhere] * len(operands),
         out_specs=(vmem, vmem),
         scratch_shapes=[pltpu.VMEM(a.shape, a.dtype) for a in operands] + [
             pltpu.VMEM((4, merged), f32),
@@ -723,10 +749,7 @@
             collective_id=0, has_side_effects=True, vmem_limit_bytes=56 * 1024 * 1024
         ),
         name="fused",
-    )(
-        routes.T, route_weight.T, log_step.reshape(1, groups), norm_gain.reshape(1, features),
-        *operands,
-    ))
+    )(*operands))
 
 
 def solution(mesh):

time: 60.6 us -> 59.6 us (0.983)
  Pallas kernels: 58.4 us -> 57.5 us
    pallas_call x1, Pallas kernels: 58.4 us -> 57.5 us  [shards(): pl.pallas_call(functools.partial(fused_kernel, n_ep, n_tp, states), out_s...]
where the time goes in v5:
time: 59.6 us; the launch traced here: 59.5 us
  Pallas kernels  57.5 us (96%)
  local copies, waits for them, and re-layouts  1.36 us (2%)
  between operations  0.65 us (1%)
    pallas_call x1, Pallas kernels, shards(): pl.pallas_call(functools.partial(fused_kernel, n_ep, n_tp, states), out_s...  57.5 us
    unnamed x2, local copies, waits for them, and re-layouts  1.36 us

profile of v5, /device:TPU:1, one launch (start us, length us, event | category | flops | bytes accessed | tf_op | source)
XLA Modules:
  0.0 59.5 jit_solution(7779333566630146281)
XLA Ops:
  0.6 57.5 %fused.1 = (bf16[256,512]{1,0:T(8,128)(2,1)S(1)}, bf16[128,512]{1,0:T(8,128)(2,1)S(1)}) custom-call(s32[2,128]{1,0:T(2,128)} %bitcast.21, f32[2,128]{1,0:T(2,128)} %bitcast.22, f32[1,16]{1,0:T(1,128)} %bitcast.23, f32[1,2048]{1,0:T(1,128)} %bitcast.20, bf16[2,64,2048]{2,1,0:T(8,128)(2,1)} %bitcast.16, bf16[256,256]{1,0:T(8,128)(2,1)} %x_hbm.1, ...), custom_call_target="tpu_custom_call" | custom-call | tf_op jit(solution)/shard_map/fused/pallas_call | solution.py:715
  58.1 0.7 %copy.20 = bf16[256,512]{1,0:T(8,128)(2,1)} copy(bf16[256,512]{1,0:T(8,128)(2,1)S(1)} %get-tuple-element.2) | data formatting | bytes 524288
  58.8 0.7 %copy.21 = bf16[128,512]{1,0:T(8,128)(2,1)} copy(bf16[128,512]{1,0:T(8,128)(2,1)S(1)} %get-tuple-element.3) | data formatting | bytes 262144

commit v6 on v5

--- a/solution.py
+++ b/solution.py
@@ -597,6 +597,11 @@
         arrivals(3 * u)
         if 1 < u == last:
             forward(groups[u])
+        elif u == last - 1 > 1:
+            @pl.when(end)
+            def _():
+                forward(groups[u])
+
         ready(source[u])
         process(source[u])
         arrivals(3 * u + 1)
@@ -607,6 +612,11 @@
 
             scan_states()
 
+            @pl.when(jnp.logical_not(end))
+            def _():
+                forward(groups[u])
+
+        elif u == last - 1:
             @pl.when(jnp.logical_not(end))
             def _():
                 forward(groups[u])

time: 59.6 us -> 59.6 us (level)
  no operation moved by 1% of the time
where the time goes in v6:
time: 59.6 us; the launch traced here: 59.5 us
  Pallas kernels  57.5 us (96%)
  local copies, waits for them, and re-layouts  1.36 us (2%)
  between operations  0.65 us (1%)
    pallas_call x1, Pallas kernels, shards(): pl.pallas_call(functools.partial(fused_kernel, n_ep, n_tp, states), out_s...  57.5 us
    unnamed x2, local copies, waits for them, and re-layouts  1.36 us

profile of v6, /device:TPU:1, one launch (start us, length us, event | category | flops | bytes accessed | tf_op | source)
XLA Modules:
  0.0 59.5 jit_solution(16729281431692523424)
XLA Ops:
  0.6 57.5 %fused.1 = (bf16[256,512]{1,0:T(8,128)(2,1)S(1)}, bf16[128,512]{1,0:T(8,128)(2,1)S(1)}) custom-call(s32[2,128]{1,0:T(2,128)} %bitcast.21, f32[2,128]{1,0:T(2,128)} %bitcast.22, f32[1,16]{1,0:T(1,128)} %bitcast.23, f32[1,2048]{1,0:T(1,128)} %bitcast.20, bf16[2,64,2048]{2,1,0:T(8,128)(2,1)} %bitcast.16, bf16[256,256]{1,0:T(8,128)(2,1)} %x_hbm.1, ...), custom_call_target="tpu_custom_call" | custom-call | tf_op jit(solution)/shard_map/fused/pallas_call | solution.py:725
  58.1 0.7 %copy.20 = bf16[256,512]{1,0:T(8,128)(2,1)} copy(bf16[256,512]{1,0:T(8,128)(2,1)S(1)} %get-tuple-element.2) | data formatting | bytes 524288
  58.8 0.7 %copy.21 = bf16[128,512]{1,0:T(8,128)(2,1)} copy(bf16[128,512]{1,0:T(8,128)(2,1)S(1)} %get-tuple-element.3) | data formatting | bytes 262144
